TPU v7x, 512 devices: a whole 4x4x16 slice. The times are simulated.
512 devices in a mesh: sp: 32 (over z, core), tp: 16 (over y, x).
Axes of the slice: x: 4, y: 4, z: 16, core: 2. Of those that a mesh axis runs over, the one named last changes fastest.
Arguments:
- mixer_in: bfloat16 [2048, 2048], P('sp', 'tp'), may hold values from -6 to 6
- residual: bfloat16 [2048, 2048], P('sp', 'tp')
- doc_ids: int32 [2048], P('sp'), may hold values from 0 to 7, never falling along the last dimension, each value on 1 to 1280 neighbouring positions
- log_step: float32 [2, 128], P(None, 'tp'), as said below
- log_extra: float32 [2048, 128], P('sp', 'tp'), as said below
- in_mix: float32 [2, 128, 16, 128], P(None, 'tp'), may hold values from -1.5 to 1.5
- read_mix: float32 [2, 128, 128, 16], P(None, 'tp'), may hold values from -0.5 to 0.5
- skip_gain: float32 [2048], P('tp'), may hold values from -4 to 4
- out_weight: bfloat16 [2048, 2048], P('tp'), may hold values from -0.1875 to 0.1875
- norm_gain: float32 [2048], P('tp'), may hold values from 0.1 to 1.9
- routes: int32 [2048, 2], P('sp'), may hold values from 0 to 31, all different within a row; in each aligned block of 64 rows (0 to 63, 64 to 127, ...) at most 5 rows name the same one
- route_weight: float32 [2048, 2], P('sp'), may hold values from 0.25 to 1
- switch_matrices: bfloat16 [32, 2048, 4096], P('sp', None, 'tp'), may hold values from -0.125 to 0.125
- up_weight: bfloat16 [32, 2048, 4096], P('sp', None, 'tp'), may hold values from -0.125 to 0.125
- down_weight: bfloat16 [32, 4096, 2048], P('sp', 'tp'), may hold values from -0.125 to 0.125
Outputs:
- layer_out: bfloat16 [2048, 2048], P('sp', 'tp')
Inputs may be any that keep to these rules, and one draw needn't show every extreme that they name: In each aligned block of 64 rows no expert is named by more than 5 routes, a bound that some block reaches; each row names 2 different experts. `doc_ids`: document numbers never fall; each document is a run of positions and one has exactly 1280 positions. `log_step`: logarithms of positive step sizes. `log_extra`: every entry is at most zero.
All inputs are finite; a program needn't handle non-finite values.
Results may differ from a plain program's by a relative error of at most 0.014.
Values may be sent and summed in bfloat16 or wider, within the bound.
No kernel may reach another device: no remote copies, remote signals or barrier semaphores. Data moves between devices by JAX's collectives and lax.ppermute only.
A program may use at most 64 MiB of HBM per device.

v0:
```python
import functools

import jax
import jax.numpy as jnp
from jax import lax
from jax.sharding import Mesh
from jax.sharding import PartitionSpec as P

D = 2048
TOP = 2
TP = ("tp_0", "tp_1")


epsilon = 1e-06


def copy_for_each(shard, axis):
    devices = lax.axis_size(axis)
    return lax.all_to_all(
        jnp.broadcast_to(shard[None], (devices, *shard.shape)), axis, 0, 0, tiled=True
    )


def collected_together(shard, axis):
    leaves = jax.tree.leaves(shard)
    order = sorted(range(len(leaves)), key=lambda k: -leaves[k].size)
    width = (1, *leaves[order[0]].shape)[-1]
    lines = [
        jnp.pad(leaves[k].reshape(-1), (0, -leaves[k].size % width)).reshape(-1, width)
        for k in order
    ]
    both, at, found = (copy_for_each(jnp.concatenate(lines), axis), 0, {})
    for k, line in zip(order, lines):
        piece = both[:, at : at + len(line)].reshape(len(both), -1)
        found[k] = piece[:, : leaves[k].size].reshape(-1, *leaves[k].shape)
        at += len(line)
    numbers = iter(range(len(leaves)))
    return jax.tree.map(lambda _: found[next(numbers)], shard)


def folded_in_pairs(pieces, combine):
    while len(jax.tree.leaves(pieces)[0]) > 1:
        pieces = jax.vmap(combine)(
            *(jax.tree.map(lambda part: part[side::2], pieces) for side in (0, 1))
        )
    return jax.tree.map(lambda part: part[0], pieces)


def carried_in(shard, axis, combine, identity, reverse):
    devices, index = (lax.axis_size(axis), lax.axis_index(axis))
    passed = jnp.arange(devices) > index if reverse else jnp.arange(devices) < index

    def kept(part, zero, own):
        part = jnp.where(
            passed.reshape(-1, *(1 for _ in own.shape)), part, jnp.asarray(zero, own.dtype)
        )
        return part[::-1] if reverse else part

    pieces = collected_together(shard, axis)
    return folded_in_pairs(jax.tree.map(kept, pieces, identity, shard), combine)


def cut_along(shard, dim, devices):
    shape = shard.shape
    tiles = shard.reshape(*shape[:dim], devices, shape[dim] // devices, *shape[dim + 1 :])
    return jnp.moveaxis(tiles, dim, 0)


def summed_on_arrival(shard, axis, dim):
    devices = lax.axis_size(axis)
    tiles = lax.all_to_all(cut_along(shard, dim, devices), axis, 0, 0, tiled=True)
    return jnp.sum(tiles.astype(jnp.float32), axis=0)


def by_axis(shard, axes):
    return functools.reduce(lax.psum, axes, shard)


def joined_along(tiles, dim):
    tiles = jnp.moveaxis(tiles, 0, dim)
    shape = tiles.shape
    return tiles.reshape(*shape[:dim], shape[dim] * shape[dim + 1], *shape[dim + 2 :])


def gather_directly(shard, axis, dim):
    return joined_along(copy_for_each(shard, axis), dim)


def complex_product(former, latter):
    return (
        former[0] * latter[0] - former[1] * latter[1],
        former[0] * latter[1] + former[1] * latter[0],
    )


def carry_join(earlier, latter):
    linked = jnp.where((earlier[5] == latter[4]) | (earlier[5] < 0.0) | (latter[4] < 0.0), 1.0, 0.0)
    decay_pair = complex_product((latter[0], latter[1]), (earlier[0], earlier[1]))
    carried = complex_product((latter[0], latter[1]), (earlier[2], earlier[3]))
    entry_seg = jnp.where(earlier[4] < 0.0, latter[4], earlier[4])
    leave_seg = jnp.where(latter[5] < 0.0, earlier[5], latter[5])
    return (
        decay_pair[0] * linked,
        decay_pair[1] * linked,
        carried[0] * linked + latter[2],
        carried[1] * linked + latter[3],
        entry_seg,
        leave_seg,
    )


def chain_step(carried, current):
    decay_now = complex_product((current[0], current[1]), (carried[0], carried[1]))
    state_now = complex_product((current[0], current[1]), (carried[2], carried[3]))
    updated = (decay_now[0], decay_now[1], state_now[0] + current[2], state_now[1] + current[3])
    return updated


def run_chain(decay_pair, source_input, backward):
    row_count, state_width = decay_pair[0].shape
    lane_count = 16
    step_count = row_count // lane_count

    def fold_lanes(member):
        return jnp.swapaxes(member.reshape(lane_count, step_count, state_width), 0, 1)

    def spread_back(member):
        return jnp.swapaxes(member, 0, 1).reshape(row_count, state_width)

    members = tuple(
        (
            fold_lanes(member)
            for member in (decay_pair[0], decay_pair[1], source_input[0], source_input[1])
        )
    )

    def within(carried, current):
        updated = chain_step(carried, current)
        return (updated, updated)

    unit_lanes = jnp.ones((lane_count, state_width), jnp.float32)
    empty_lanes = jnp.zeros((lane_count, state_width), jnp.float32)
    unused, lane_runs = lax.scan(
        within, (unit_lanes, empty_lanes, empty_lanes, empty_lanes), members, reverse=backward
    )
    edge_index = 0 if backward else step_count - 1
    lane_totals = tuple((member[edge_index] for member in lane_runs))

    def across(carried, current):
        return (chain_step(carried, current), carried)

    unit_state = jnp.ones((state_width,), jnp.float32)
    empty_state = jnp.zeros((state_width,), jnp.float32)
    unused_total, incoming = lax.scan(
        across, (unit_state, empty_state, empty_state, empty_state), lane_totals, reverse=backward
    )
    decay_run = complex_product(
        (lane_runs[0], lane_runs[1]), (incoming[0][None], incoming[1][None])
    )
    carried_state = complex_product(
        (lane_runs[0], lane_runs[1]), (incoming[2][None], incoming[3][None])
    )
    states = (lane_runs[2] + carried_state[0], lane_runs[3] + carried_state[1])
    return (
        (spread_back(decay_run[0]), spread_back(decay_run[1])),
        (spread_back(states[0]), spread_back(states[1])),
    )


def local_sweep(inputs, magnitude, step_size, weights, backward):
    states_count = weights.shape[2] // 2
    row_count = inputs.shape[0]
    phase_angle = (
        jnp.pi * jnp.arange(states_count, dtype=jnp.float32)[None, :] * step_size[:, None]
    ).reshape(-1)
    spread = jnp.repeat(magnitude, states_count, axis=1)
    decay_pair = (spread * jnp.cos(phase_angle)[None, :], spread * jnp.sin(phase_angle)[None, :])
    projected = jnp.einsum("tgh,ghq->tgq", inputs, weights)
    input_scale = jnp.sqrt(-jnp.expm1(-step_size))[None, :, None]
    source_input = (
        (input_scale * projected[:, :, :states_count]).reshape(row_count, -1),
        (input_scale * projected[:, :, states_count:]).reshape(row_count, -1),
    )
    return run_chain(decay_pair, source_input, backward)


def settle(decay_run, local_states, carried, edge_seg):
    linked = (carried[5] == edge_seg).astype(jnp.float32)
    incoming = complex_product(decay_run, (carried[2] * linked, carried[3] * linked))
    return (local_states[0] + incoming[0], local_states[1] + incoming[1])


def read_states(states, weights, groups):
    row_count = states[0].shape[0]
    stacked = jnp.concatenate(
        [states[0].reshape(row_count, groups, -1), states[1].reshape(row_count, groups, -1)], axis=2
    )
    return jnp.einsum("tgq,gqh->tgh", stacked, weights).reshape(row_count, -1)


def shards(
    mixer_in,
    residual,
    doc_ids,
    log_step,
    log_extra,
    in_mix,
    read_mix,
    skip_gain,
    out_weight,
    norm_gain,
    routes,
    route_weight,
    switch_matrices,
    up_weight,
    down_weight,
):
    row_count = mixer_in.shape[0]
    channels = mixer_in.shape[1]
    groups = log_step.shape[1]
    inputs = mixer_in.astype(jnp.float32).reshape(row_count, groups, channels // groups)
    seg_float = doc_ids.astype(jnp.float32)
    single_one = jnp.ones((1,), jnp.float32)
    same_prev = jnp.concatenate([single_one, (seg_float[1:] == seg_float[:-1]).astype(jnp.float32)])
    same_next = jnp.concatenate([(seg_float[:-1] == seg_float[1:]).astype(jnp.float32), single_one])
    step_size = jnp.exp(log_step)
    magnitude_fwd = jnp.exp(-0.5 * step_size[0][None, :] + log_extra) * same_prev[:, None]
    magnitude_bwd = jnp.exp(-0.5 * step_size[1][None, :] + log_extra) * same_next[:, None]
    run_fwd, local_fwd = local_sweep(inputs, magnitude_fwd, step_size[0], in_mix[0], False)
    run_bwd, local_bwd = local_sweep(inputs, magnitude_bwd, step_size[1], in_mix[1], True)
    first_seg = seg_float[:1]
    last_seg = seg_float[-1:]
    summary_fwd = (
        run_fwd[0][-1],
        run_fwd[1][-1],
        local_fwd[0][-1],
        local_fwd[1][-1],
        first_seg,
        last_seg,
    )
    summary_bwd = (
        run_bwd[0][0],
        run_bwd[1][0],
        local_bwd[0][0],
        local_bwd[1][0],
        last_seg,
        first_seg,
    )
    state_width = run_fwd[0].shape[1]
    zero_state = jnp.zeros((state_width,), jnp.float32)
    identity = (
        jnp.ones((state_width,), jnp.float32),
        zero_state,
        zero_state,
        zero_state,
        -single_one,
        -single_one,
    )
    carry_fwd = carried_in(summary_fwd, "sp", carry_join, identity, False)
    carry_bwd = carried_in(summary_bwd, "sp", carry_join, identity, True)
    states_fwd = settle(run_fwd, local_fwd, carry_fwd, first_seg)
    states_bwd = settle(run_bwd, local_bwd, carry_bwd, last_seg)
    mixed = (
        skip_gain[None, :] * mixer_in.astype(jnp.float32)
        + read_states(states_fwd, read_mix[0], groups)
        + read_states(states_bwd, read_mix[1], groups)
    )
    activated = jax.nn.gelu(mixed).astype(jnp.bfloat16)
    partial_sum = jnp.dot(activated, out_weight, preferred_element_type=jnp.float32)
    projected = summed_on_arrival(partial_sum.astype(jnp.bfloat16), TP, 1)
    stream = (residual.astype(jnp.float32) + projected).astype(jnp.bfloat16)
    stream_values = stream.astype(jnp.float32)
    squares = by_axis(jnp.sum(stream_values * stream_values, axis=1), TP)
    normed = (
        stream_values * lax.rsqrt(squares / D + epsilon)[:, None] * norm_gain[None, :]
    ).astype(jnp.bfloat16)
    experts_total = lax.axis_size("sp")
    capacity = row_count * TOP * 5 // (4 * experts_total)
    flat_routes = routes.reshape(-1)
    onehot = (flat_routes[:, None] == jnp.arange(experts_total, dtype=jnp.int32)[None, :]).astype(
        jnp.int32
    )
    slot_rank = jnp.sum((jnp.cumsum(onehot, axis=0) - 1) * onehot, axis=1)
    slot_ids = flat_routes * capacity + slot_rank
    slot_table = jnp.arange(experts_total * capacity, dtype=jnp.int32)
    placing = jnp.any(
        (slot_table[:, None] == slot_ids[None, :]).reshape(
            experts_total * capacity, row_count, TOP
        ),
        axis=2,
    ).astype(jnp.bfloat16)
    outgoing = (
        jnp.dot(placing, normed, preferred_element_type=jnp.float32)
        .astype(jnp.bfloat16)
        .reshape(experts_total, capacity, -1)
    )
    arrived = lax.all_to_all(outgoing, "sp", split_axis=0, concat_axis=0, tiled=True)
    total_rows = arrived.shape[0] * arrived.shape[1]
    segment_piece = gather_directly(arrived, TP, 2)
    piece_rows = segment_piece.reshape(total_rows, segment_piece.shape[2])
    gate_rows = switch_matrices[0]
    up_rows = up_weight[0]
    gate_acts = jnp.dot(piece_rows, gate_rows, preferred_element_type=jnp.float32)
    up_acts = jnp.dot(piece_rows, up_rows, preferred_element_type=jnp.float32)
    hidden = (jax.nn.silu(gate_acts) * up_acts).astype(jnp.bfloat16)
    expert_terms = jnp.dot(hidden, down_weight[0], preferred_element_type=jnp.float32).reshape(
        experts_total, capacity, -1
    )
    expert_out = summed_on_arrival(expert_terms.astype(jnp.bfloat16), TP, 2).astype(jnp.bfloat16)
    returned = lax.all_to_all(expert_out, "sp", split_axis=0, concat_axis=0, tiled=True)
    returned_rows = returned.reshape(experts_total * capacity, -1)
    picked = returned_rows[slot_ids].reshape(row_count, TOP, -1)
    mixture = jnp.sum(picked.astype(jnp.float32) * route_weight[:, :, None], axis=1)
    return (stream_values + mixture).astype(jnp.bfloat16)


def solution(mesh):
    split = Mesh(mesh.devices.reshape(mesh.shape["sp"], 4, 4), ("sp", "tp_0", "tp_1"))
    in_specs = (
        P("sp", TP),
        P("sp", TP),
        P("sp"),
        P(None, TP),
        P("sp", TP),
        P(None, TP, None, None),
        P(None, TP, None, None),
        P(TP),
        P(TP, None),
        P(TP),
        P("sp", None),
        P("sp", None),
        P("sp", None, TP),
        P("sp", None, TP),
        P("sp", TP, None),
    )
    out_specs = P("sp", TP)
    return jax.shard_map(
        shards, mesh=split, in_specs=in_specs, out_specs=out_specs, check_vma=False
    )
```

profile of v0, /device:TPU:1, one launch (start us, length us, event | category | flops | bytes accessed | tf_op | source)
XLA Modules:
  0.0 234.2 jit_solution(10032156745425207366)
XLA Ops:
  0.0 0.8 exp.13
  0.8 0.8 copy.254
  1.6 1.1 convolution_bitcast_fusion
  2.7 1.1 convolution_bitcast_fusion.1
  3.9 0.7 convert_element_type.63
  5.3 0.8 exponential_multiply_fusion.1
  7.7 0.9 while.108
  8.7 6.3 %while.109 = (s32[]{:T(128)}, f32[512]{0:T(512)S(1)}, f32[512]{0:T(512)S(1)}, f32[512]{0:T(512)S(1)}, f32[512]{0:T(512)S(1)}, /*index=5*/f32[16,512]{1,0:T(8,128...) while((s32[]{:T(128)}, f32[512]{0:T(512)S(1)}, ...), condition=%wide.region_3.4_spmd.clone, body=%wide.region_2.3_spmd.clone.sunk | while | flops 9219 | bytes 82096 | solution.py:154
  15.8 0.7 pad.9
  16.5 0.7 pad.10
  17.2 0.9 broadcast_in_dim.271
  18.1 16.7 %all-to-all-start = ((f32[32,6,512]{2,1,0:T(8,128)}), f32[32,6,512]{2,1,0:T(8,128)S(1)}, u32[]{:S(2)}, u32[]{:S(2)}) async-start(f32[32,6,512]{2,1,0:T(8,128)} %broadcast_in_dim.271), calls=%async_computation | async-start | bytes 1048576 | tf_op jit(solution)/shard_map/all_to_all | solution.py:19
  36.1 0.9 while.110
  37.1 6.3 %while.111 = (s32[]{:T(128)}, f32[512]{0:T(512)S(1)}, f32[512]{0:T(512)S(1)}, f32[512]{0:T(512)S(1)}, f32[512]{0:T(512)S(1)}, /*index=5*/f32[16,512]{1,0:T(8,128...) while((s32[]{:T(128)}, f32[512]{0:T(512)S(1)}, ...), condition=%wide.region_7.8_spmd.clone, body=%wide.region_6.7_spmd.clone.sunk | while | flops 9220 | bytes 82116 | solution.py:154
  43.6 0.8 reshape.377
  44.5 0.8 reshape.390
  45.3 0.8 reshape.391
  48.1 0.8 reduce_sum.54
  48.9 19.4 %all-to-all-done = f32[32,6,512]{2,1,0:T(8,128)S(1)} async-done(((f32[32,6,512]{2,1,0:T(8,128)}), f32[32,6,512]{2,1,0:T(8,128)S(1)}, u32[]{:S(2)}, u32[]{:S(2)}) %all-to-all-start) | async-done | bytes 393248 | tf_op jit(solution)/shard_map/all_to_all | solution.py:19
  68.3 0.9 broadcast_in_dim.281
  69.2 4.0 %all-to-all-start.1 = ((f32[32,6,512]{2,1,0:T(8,128)}), f32[32,6,512]{2,1,0:T(8,128)S(1)}, u32[]{:S(2)}, u32[]{:S(2)}) async-start(f32[32,6,512]{2,1,0:T(8,128)} %broadcast_in_dim.281), calls=%async_computation.1 | async-start | bytes 1048576 | tf_op jit(solution)/shard_map/all_to_all | solution.py:19
  73.2 1.0 fusion.85
  74.3 0.8 copy.466
  80.0 1.0 fusion.31
  84.3 22.5 %all-to-all-done.1 = f32[32,6,512]{2,1,0:T(8,128)S(1)} async-done(((f32[32,6,512]{2,1,0:T(8,128)}), f32[32,6,512]{2,1,0:T(8,128)S(1)}, u32[]{:S(2)}, u32[]{:S(2)}) %all-to-all-start.1) | async-done | bytes 393248 | tf_op jit(solution)/shard_map/all_to_all | solution.py:19
  107.2 0.7 compare_select_fusion.1
  107.9 0.7 compare_select_fusion.5
  114.7 0.7 subtract_multiply_fusion
  115.6 0.7 subtract_multiply_fusion.2
  116.5 0.7 subtract_multiply_fusion.4
  119.9 1.3 slice.728
  121.1 1.3 subtract_multiply_fusion.7
  122.5 0.8 multiply_add_fusion.18
  127.0 0.7 subtract_multiply_fusion.6
  128.8 0.8 copy.462
  129.5 6.8 %all-to-all-start.2 = ((bf16[16,64,128]{2,1,0:T(8,128)(2,1)}), bf16[16,64,128]{2,1,0:T(8,128)(2,1)S(1)}, u32[]{:S(2)}, u32[]{:S(2)}) async-start(bf16[16,64,128]{2,1,0:T(8,128)(2,1)} %bitcast.278), calls=%async_computation.2 | async-start | bytes 524288 | tf_op jit(solution)/shard_map/all_to_all | solution.py:71
  136.5 7.3 %all-to-all-done.2 = bf16[16,64,128]{2,1,0:T(8,128)(2,1)S(1)} async-done(((bf16[16,64,128]{2,1,0:T(8,128)(2,1)}), bf16[16,64,128]{2,1,0:T(8,128)(2,1)S(1)}, u32[]{:S(2)}, u32[]{:S(2)}) %all-to-all-start.2) | async-done | bytes 262176 | tf_op jit(solution)/shard_map/all_to_all | solution.py:71
  144.0 6.9 %psum.14 = f32[64]{0:T(128)S(1)} all-reduce(f32[64]{0:T(128)S(1)} %get-tuple-element.1111), channel_id=1, replica_groups=mesh['sp'=32,'tp_0'=4,'tp_1'=4] {'tp_0'}, use_global_device_ids=true, to_apply=%region_13.14 | all-reduce | flops 64 | bytes 512 | tf_op jit(solution)/shard_map/psum | solution.py:76
  150.9 6.6 %psum.15 = f32[64]{0:T(128)S(1)} all-reduce(f32[64]{0:T(128)S(1)} %psum.14), channel_id=1, replica_groups=mesh['sp'=32,'tp_0'=4,'tp_1'=4] {'tp_1'}, use_global_device_ids=true, to_apply=%region_14.15 | all-reduce | flops 64 | bytes 512 | tf_op jit(solution)/shard_map/psum | solution.py:76
  157.7 21.9 %all_to_all.35 = bf16[32,5,128]{2,1,0:T(8,128)(2,1)S(1)} all-to-all(bf16[32,5,128]{2,1,0:T(8,128)(2,1)S(1)} %reshape.410), channel_id=1, replica_groups=mesh['sp'=32,'tp_0'=4,'tp_1'=4] {'sp'}, dimensions={0} | all-to-all | bytes 81920 | tf_op jit(solution)/shard_map/all_to_all | solution.py:297
  179.8 14.0 %all_to_all.36 = bf16[16,32,5,128]{3,1,2,0:T(8,128)(2,1)S(1)} all-to-all(bf16[16,32,5,128]{3,1,2,0:T(8,128)(2,1)S(1)} %broadcast_in_dim.282), channel_id=1, replica_groups=mesh['sp'=32,'tp_0'=4,'tp_1'=4] {'tp_0','tp_1'}, dimensions={0} | all-to-all | bytes 1310720 | tf_op jit(solution)/shard_map/all_to_all | solution.py:19
  194.4 0.9 copy-done.18
  196.0 1.0 copy.461
  196.9 3.7 %all-to-all-start.5 = ((bf16[16,32,5,128]{3,1,2,0:T(8,128)(2,1)}), bf16[16,32,5,128]{3,1,2,0:T(8,128)(2,1)S(1)}, u32[]{:S(2)}, u32[]{:S(2)}) async-start(bf16[16,32,5,128]{3,1,2,0:T(8,128)(2,1)} %bitcast.276), calls=%async_computation.5 | async-start | bytes 1310720 | tf_op jit(solution)/shard_map/all_to_all | solution.py:71
  200.8 10.5 %all-to-all-done.5 = bf16[16,32,5,128]{3,1,2,0:T(8,128)(2,1)S(1)} async-done(((bf16[16,32,5,128]{3,1,2,0:T(8,128)(2,1)}), bf16[16,32,5,128]{3,1,2,0:T(8,128)(2,1)S(1)}, u32[]{:S(2)}, u32[]{:S(2)}) %all-to-all-start.5) | async-done | bytes 655392 | tf_op jit(solution)/shard_map/all_to_all | solution.py:71
  212.0 7.7 %all-to-all-start.6 = ((bf16[32,5,128]{2,1,0:T(8,128)(2,1)}), bf16[32,5,128]{2,1,0:T(8,128)(2,1)S(1)}, u32[]{:S(2)}, u32[]{:S(2)}) async-start(bf16[32,5,128]{2,1,0:T(8,128)(2,1)} %copy.317), calls=%async_computation.6 | async-start | bytes 131072 | tf_op jit(solution)/shard_map/all_to_all | solution.py:310
  219.9 12.9 %all-to-all-done.6 = bf16[32,5,128]{2,1,0:T(8,128)(2,1)S(1)} async-done(((bf16[32,5,128]{2,1,0:T(8,128)(2,1)}), bf16[32,5,128]{2,1,0:T(8,128)(2,1)S(1)}, u32[]{:S(2)}, u32[]{:S(2)}) %all-to-all-start.6) | async-done | bytes 40992 | tf_op jit(solution)/shard_map/all_to_all | solution.py:310
  232.8 0.7 gather_fusion
  (628 shorter events, 34.1 us)
Async XLA Ops:
  0.0 195.6 %copy-start = (bf16[1,256,2048]{2,1,0:T(8,128)(2,1)S(1)}, bf16[1,256,2048]{2,1,0:T(8,128)(2,1)}, u32[]{:S(2)}) copy-start(bf16[1,256,2048]{2,1,0:T(8,128)(2,1)} %param.37) | copy-start | bytes 3145732
  18.1 50.3 %all-to-all-start = ((f32[32,6,512]{2,1,0:T(8,128)}), f32[32,6,512]{2,1,0:T(8,128)S(1)}, u32[]{:S(2)}, u32[]{:S(2)}) async-start(f32[32,6,512]{2,1,0:T(8,128)} %broadcast_in_dim.271), calls=%async_computation | async-start | bytes 1048576 | tf_op jit(solution)/shard_map/all_to_all | solution.py:19
  46.6 0.8 copy-start.15
  47.5 26.7 %copy-start.6 = (s32[64,2]{1,0:T(8,128)}, s32[64,2]{1,0:T(8,128)S(1)}, u32[]{:S(2)}) copy-start(s32[64,2]{1,0:T(8,128)S(1)} %copy.309) | copy-start | bytes 1540
  48.1 26.1 %copy-start.12 = (s32[128]{0:T(128)}, s32[128]{0:T(128)S(1)}, u32[]{:S(2)}) copy-start(s32[128]{0:T(128)S(1)} %select_reduce_fusion) | copy-start | bytes 1540
  69.2 37.6 %all-to-all-start.1 = ((f32[32,6,512]{2,1,0:T(8,128)}), f32[32,6,512]{2,1,0:T(8,128)S(1)}, u32[]{:S(2)}, u32[]{:S(2)}) async-start(f32[32,6,512]{2,1,0:T(8,128)} %broadcast_in_dim.281), calls=%async_computation.1 | async-start | bytes 1048576 | tf_op jit(solution)/shard_map/all_to_all | solution.py:19
  113.7 9.7 %copy-start.2 = (f32[64,8,64]{2,1,0:T(8,128)S(1)}, f32[64,8,64]{2,1,0:T(8,128)}, u32[]{:S(2)}) copy-start(f32[64,8,64]{2,1,0:T(8,128)} %reshape.377) | copy-start | bytes 393220
  113.7 9.7 %copy-start.3 = (f32[64,8,64]{2,1,0:T(8,128)S(1)}, f32[64,8,64]{2,1,0:T(8,128)}, u32[]{:S(2)}) copy-start(f32[64,8,64]{2,1,0:T(8,128)} %reshape.390) | copy-start | bytes 393220
  113.7 9.7 %copy-start.4 = (f32[64,8,64]{2,1,0:T(8,128)S(1)}, f32[64,8,64]{2,1,0:T(8,128)}, u32[]{:S(2)}) copy-start(f32[64,8,64]{2,1,0:T(8,128)} %reshape.391) | copy-start | bytes 393220
  115.5 8.1 %copy-start.9 = (f32[2,8,128,16]{2,3,1,0:T(8,128)S(1)}, f32[2,8,128,16]{2,3,1,0:T(8,128)}, u32[]{:S(2)}) copy-start(f32[2,8,128,16]{2,3,1,0:T(8,128)} %param.29) | copy-start | bytes 393220
  116.5 10.0 %copy-start.14 = (f32[2]{0:T(128)S(1)}, f32[2]{0:T(128)}, u32[]{:S(2)}) copy-start(f32[2]{0:T(128)} %get-tuple-element.1263) | copy-start | bytes 28
  123.9 4.6 %copy-start.5 = (bf16[128,2048]{1,0:T(8,128)(2,1)S(1)}, bf16[128,2048]{1,0:T(8,128)(2,1)}, u32[]{:S(2)}) copy-start(bf16[128,2048]{1,0:T(8,128)(2,1)} %param.31) | copy-start | bytes 1572868
  123.9 4.6 %copy-start.10 = (bf16[64,128]{1,0:T(8,128)(2,1)S(1)}, bf16[64,128]{1,0:T(8,128)(2,1)}, u32[]{:S(2)}) copy-start(bf16[64,128]{1,0:T(8,128)(2,1)} %param.23) | copy-start | bytes 49156
  123.9 4.6 %copy-start.17 = (f32[128]{0:T(128)S(1)}, f32[128]{0:T(128)}, u32[]{:S(2)}) copy-start(f32[128]{0:T(128)} %param.30) | copy-start | bytes 1540
  128.4 7.9 %copy-start.7 = (s32[64,2]{1,0:T(8,128)S(1)}, s32[64,2]{1,0:T(8,128)}, u32[]{:S(2)}) copy-start(s32[64,2]{1,0:T(8,128)} %copy-done.6) | copy-start | bytes 1540
  128.4 7.9 %copy-start.8 = (s32[64,2]{1,0:T(8,128)S(1)}, s32[64,2]{1,0:T(8,128)}, u32[]{:S(2)}) copy-start(s32[64,2]{1,0:T(8,128)} %reduce_sum.54) | copy-start | bytes 1540
  128.5 15.4 %copy-start.11 = (bf16[64,128]{1,0:T(8,128)(2,1)S(1)}, bf16[64,128]{1,0:T(8,128)(2,1)}, u32[]{:S(2)}) copy-start(bf16[64,128]{1,0:T(8,128)(2,1)} %param.24) | copy-start | bytes 49156
  128.5 28.9 %copy-start.19 = (f32[128]{0:T(128)S(1)}, f32[128]{0:T(128)}, u32[]{:S(2)}) copy-start(f32[128]{0:T(128)} %param.32) | copy-start | bytes 1540
  129.5 14.3 %all-to-all-start.2 = ((bf16[16,64,128]{2,1,0:T(8,128)(2,1)}), bf16[16,64,128]{2,1,0:T(8,128)(2,1)S(1)}, u32[]{:S(2)}, u32[]{:S(2)}) async-start(bf16[16,64,128]{2,1,0:T(8,128)(2,1)} %bitcast.278), calls=%async_computation.2 | async-start | bytes 524288 | tf_op jit(solution)/shard_map/all_to_all | solution.py:71
  179.7 14.3 %copy-start.1 = (bf16[1,2048,256]{2,1,0:T(8,128)(2,1)S(1)}, bf16[1,2048,256]{2,1,0:T(8,128)(2,1)}, u32[]{:S(2)}) copy-start(bf16[1,2048,256]{2,1,0:T(8,128)(2,1)} %param.35) | copy-start | bytes 3145732
  194.0 1.2 copy-start.18
  196.9 22.8 %copy-start.13 = (s32[128]{0:T(128)S(1)}, s32[128]{0:T(128)}, u32[]{:S(2)}) copy-start(s32[128]{0:T(128)} %copy-done.12) | copy-start | bytes 1540
  196.9 22.8 %copy-start.16 = (f32[64,2]{0,1:T(2,128)S(1)}, f32[64,2]{0,1:T(2,128)}, u32[]{:S(2)}) copy-start(f32[64,2]{0,1:T(2,128)} %param.34) | copy-start | bytes 1540
  196.9 14.3 %all-to-all-start.5 = ((bf16[16,32,5,128]{3,1,2,0:T(8,128)(2,1)}), bf16[16,32,5,128]{3,1,2,0:T(8,128)(2,1)S(1)}, u32[]{:S(2)}, u32[]{:S(2)}) async-start(bf16[16,32,5,128]{3,1,2,0:T(8,128)(2,1)} %bitcast.276), calls=%async_computation.5 | async-start | bytes 1310720 | tf_op jit(solution)/shard_map/all_to_all | solution.py:71
  212.0 20.7 %all-to-all-start.6 = ((bf16[32,5,128]{2,1,0:T(8,128)(2,1)}), bf16[32,5,128]{2,1,0:T(8,128)(2,1)S(1)}, u32[]{:S(2)}, u32[]{:S(2)}) async-start(bf16[32,5,128]{2,1,0:T(8,128)(2,1)} %copy.317), calls=%async_computation.6 | async-start | bytes 131072 | tf_op jit(solution)/shard_map/all_to_all | solution.py:310
where the time goes:
time: 235 us; the launch traced here: 234 us
  waiting for transfers between devices  72.5 us (31%)
  blocking collectives  49.3 us (21%)
  local copies, waits for them, and re-layouts  39.4 us (17%)
  starting transfers between devices  39 us (17%)
  other arithmetic  15.7 us (7%)
  between operations  11.3 us (5%)
  matrix products  4.14 us (2%)
  loops' own time  2.91 us (1%)
    all_to_all x2, waiting for transfers between devices, copy_for_each(): lax.all_to_all(jnp.broadcast_to(shard[None], (devices, *shard.shape)), ax...  41.9 us
    all_to_all x1, blocking collectives, shards(): lax.all_to_all(outgoing, 'sp', split_axis=0, concat_axis=0, tiled=True)  21.9 us
    all_to_all x2, starting transfers between devices, copy_for_each(): lax.all_to_all(jnp.broadcast_to(shard[None], (devices, *shard.shape)), ax...  20.8 us
    all_to_all x2, waiting for transfers between devices, summed_on_arrival(): lax.all_to_all(cut_along(shard, dim, devices), axis, 0, 0, tiled=True)  17.8 us
    all_to_all x1, blocking collectives, copy_for_each(): lax.all_to_all(jnp.broadcast_to(shard[None], (devices, *shard.shape)), ax...  14 us
    psum x2, blocking collectives, by_axis(): return functools.reduce(lax.psum, axes, shard)  13.4 us
    all_to_all x1, waiting for transfers between devices, shards(): lax.all_to_all(expert_out, 'sp', split_axis=0, concat_axis=0, tiled=True)  12.9 us
    all_to_all x2, starting transfers between devices, summed_on_arrival(): lax.all_to_all(cut_along(shard, dim, devices), axis, 0, 0, tiled=True)  10.5 us
  transfers between devices with their start and end apart: 5, of which 5 were waited for; matrix products, arithmetic and copies ran while one was open for 9% of the time, Pallas kernels for 0%

commit v1 on v0

v1 whole, which is shorter than its diff:
```python
import jax
import jax.numpy as jnp
from jax import lax
from jax.experimental import pallas as pl
from jax.experimental.pallas import tpu as pltpu
from jax.sharding import Mesh
from jax.sharding import PartitionSpec as P

TP = ("tp_0", "tp_1")
INTERPRET = False

epsilon = 1e-06
f32 = jnp.float32
bf16 = jnp.bfloat16

BLOCKS = 32
PEERS = 16
ROWS = 64
GROUPS = 8
SLOTS = 5
PAD = 8
EROWS = BLOCKS * SLOTS
SENT = EROWS + 16

VMEM = pl.BlockSpec(memory_space=pltpu.VMEM)
SMEM = pl.BlockSpec(memory_space=pltpu.SMEM)


def call(body, in_specs, outs, scratch=()):
    return pl.pallas_call(
        body,
        in_specs=in_specs,
        out_specs=[VMEM] * len(outs),
        out_shape=[jax.ShapeDtypeStruct(shape, dtype) for shape, dtype in outs],
        scratch_shapes=[pltpu.VMEM(shape, dtype) for shape, dtype in scratch],
        interpret=INTERPRET,
    )


def iota(shape, dim):
    return lax.broadcasted_iota(jnp.int32, shape, dim)


def mm(a, b):
    return jnp.dot(a, b, preferred_element_type=f32)


def mm_across(a, b):
    return lax.dot_general(a, b, (((1,), (1,)), ((), ())), preferred_element_type=f32)


def halves_joined(first, second):
    left = iota((128, 128), 1) < 64
    return (
        jnp.where(left, first, pltpu.roll(second, 64, 1)),
        jnp.where(left, pltpu.roll(first, 64, 1), second),
    )


def steps_by_lane(log_step):
    eye = iota((GROUPS, GROUPS), 0) == iota((GROUPS, GROUPS), 1)
    step = jnp.exp(log_step)
    columns = [
        jnp.sum(
            jnp.where(eye, jnp.broadcast_to(step[k : k + 1, :], (GROUPS, GROUPS)), 0.0),
            axis=1,
            keepdims=True,
        )
        for k in range(2)
    ]
    return jnp.where(iota((GROUPS, 128), 1) < 64, columns[0], columns[1])


def one_minus_exp(x):
    series = jnp.ones_like(x)
    for n in range(9, 1, -1):
        series = 1.0 - x * (1.0 / n) * series
    return jnp.where(x < 0.5, x * series, 1.0 - jnp.exp(-x))


def sweep_body(
    me_ref, docs_ref, log_step_ref, log_extra_ref, x_ref, in_mix_ref,
    message_ref, real_ref, imag_ref, keep_ref, turn_ref,
    masked, source, magnitude,
):
    lane = iota((GROUPS, 128), 1)
    fwd = lane < 64
    step = steps_by_lane(log_step_ref[...])
    theta = (jnp.pi * (lane & 63).astype(f32)) * step
    cos, sin = jnp.cos(theta), jnp.sin(theta)
    turn_ref[0] = cos
    turn_ref[1] = sin
    scale = jnp.sqrt(one_minus_exp(step))
    wide = iota((ROWS, 128), 1)
    x = x_ref[...].astype(f32)
    for g in range(GROUPS):
        masked[pl.ds(g, ROWS, stride=GROUPS), :] = jnp.where(wide // 16 == g, x, 0.0)
    log_extra = log_extra_ref[...]
    loss = -0.5 * step
    for n in range(ROWS):
        extra = jnp.broadcast_to(log_extra[:, n : n + 1], (GROUPS, 128))
        magnitude[pl.ds(GROUPS * n, GROUPS), :] = jnp.exp(loss + extra)
    mix_real, mix_imag = halves_joined(in_mix_ref[0], in_mix_ref[1])
    rows = masked[...].astype(bf16)
    source[0] = mm(rows, mix_real.astype(bf16))
    source[1] = mm(rows, mix_imag.astype(bf16))
    real = jnp.zeros((GROUPS, 128), f32)
    imag = jnp.zeros((GROUPS, 128), f32)
    total = jnp.ones((GROUPS, 128), f32)
    for n in range(ROWS):
        r = ROWS - 1 - n
        here, there = pl.ds(GROUPS * n, GROUPS), pl.ds(GROUPS * r, GROUPS)
        keep = jnp.where(fwd, magnitude[here, :], magnitude[there, :])
        if n > 0:
            same_fwd = jnp.where(docs_ref[n] == docs_ref[n - 1], 1.0, 0.0)
            same_bwd = jnp.where(docs_ref[r] == docs_ref[r + 1], 1.0, 0.0)
            keep = keep * jnp.where(fwd, same_fwd, same_bwd)
        new_real = scale * jnp.where(fwd, source[0, here, :], source[0, there, :])
        new_imag = scale * jnp.where(fwd, source[1, here, :], source[1, there, :])
        keep_ref[n] = keep
        real_ref[n] = new_real
        imag_ref[n] = new_imag
        by_cos, by_sin = keep * cos, keep * sin
        real, imag = (
            (by_cos * real + new_real) - by_sin * imag,
            (by_sin * real + new_imag) + by_cos * imag,
        )
        total = total * keep
    crossed = pltpu.roll(total, 64, 1)
    high = crossed.astype(bf16).astype(f32)
    decay = jnp.where((lane & 32) == 0, high, crossed - high)
    first_doc = docs_ref[0].astype(f32)
    last_doc = docs_ref[ROWS - 1].astype(f32)
    to_later = jnp.concatenate(
        [jnp.where(fwd, real, decay), jnp.where(fwd, imag, last_doc)], axis=0
    ).astype(bf16)
    to_earlier = jnp.concatenate(
        [jnp.where(fwd, decay, real), jnp.where(fwd, first_doc, imag)], axis=0
    ).astype(bf16)
    me = me_ref[0]
    for i in range(BLOCKS):
        @pl.when(me < i)
        def _():
            message_ref[i] = to_later

        @pl.when(me >= i)
        def _():
            message_ref[i] = to_earlier


def mixer_body(
    me_ref, docs_ref, message_ref, real_ref, imag_ref, keep_ref, turn_ref,
    x_ref, read_mix_ref, skip_ref, out_weight_ref,
    partial_ref,
    states, read_out,
):
    lane = iota((GROUPS, 128), 1)
    fwd = lane < 64
    odd = (lane & 32) != 0
    me = me_ref[0]
    mine = jnp.where(fwd, docs_ref[0].astype(f32), docs_ref[ROWS - 1].astype(f32))
    cos, sin = turn_ref[0], turn_ref[1]
    block_cos, block_sin = cos, sin
    for _ in range(6):
        block_cos, block_sin = (
            block_cos * block_cos - block_sin * block_sin,
            2.0 * block_cos * block_sin,
        )
    real = jnp.zeros((GROUPS, 128), f32)
    imag = jnp.zeros((GROUPS, 128), f32)
    for n in range(BLOCKS - 1):
        r = BLOCKS - 1 - n
        one, two = message_ref[n].astype(f32), message_ref[r].astype(f32)
        decay = pltpu.roll(jnp.where(fwd, two[:GROUPS], one[:GROUPS]), 64, 1)
        decay = decay + jnp.where(odd, pltpu.roll(decay, 32, 1), pltpu.roll(decay, 96, 1))
        doc = pltpu.roll(jnp.where(fwd, two[GROUPS:], one[GROUPS:]), 64, 1)
        same = doc == mine
        new_real = jnp.where(same, jnp.where(fwd, one[:GROUPS], two[:GROUPS]), 0.0)
        new_imag = jnp.where(same, jnp.where(fwd, one[GROUPS:], two[GROUPS:]), 0.0)
        by_cos, by_sin = decay * block_cos, decay * block_sin
        passed = jnp.where(fwd, (n < me).astype(jnp.int32), (r > me).astype(jnp.int32)) > 0
        real, imag = (
            jnp.where(passed, (by_cos * real + new_real) - by_sin * imag, real),
            jnp.where(passed, (by_sin * real + new_imag) + by_cos * imag, imag),
        )
    for n in range(ROWS):
        r = ROWS - 1 - n
        here, there = pl.ds(GROUPS * n, GROUPS), pl.ds(GROUPS * r, GROUPS)
        keep = keep_ref[n]
        by_cos, by_sin = keep * cos, keep * sin
        real, imag = (
            (by_cos * real + real_ref[n]) - by_sin * imag,
            (by_sin * real + imag_ref[n]) + by_cos * imag,
        )
        states[0, here, 0:64] = real[:, 0:64]
        states[0, there, 64:128] = real[:, 64:128]
        states[1, here, 0:64] = imag[:, 0:64]
        states[1, there, 64:128] = imag[:, 64:128]
    read_real, read_imag = halves_joined(read_mix_ref[0], read_mix_ref[1])
    read_out[...] = mm_across(states[0].astype(bf16), read_real.astype(bf16)) + mm_across(
        states[1].astype(bf16), read_imag.astype(bf16)
    )
    wide = iota((ROWS, 128), 1)
    mixed = skip_ref[...] * x_ref[...].astype(f32)
    for g in range(GROUPS):
        mixed = mixed + jnp.where(
            wide // 16 == g, read_out[pl.ds(g, ROWS, stride=GROUPS), :], 0.0
        )
    activated = jax.nn.gelu(mixed).astype(bf16)
    partial = mm(activated, out_weight_ref[...]).astype(bf16)
    for j in range(PEERS):
        partial_ref[j] = partial[:, 128 * j : 128 * (j + 1)]


def column(row):
    eye = iota((ROWS, ROWS), 0) == iota((ROWS, ROWS), 1)
    return jnp.sum(jnp.where(eye, row, 0.0), axis=1, keepdims=True)


def slots_down(routes, k):
    before = iota((ROWS, ROWS), 1) < iota((ROWS, ROWS), 0)
    expert = column(routes[k : k + 1])
    met = (expert == routes[0:1]).astype(f32) + (expert == routes[1:2]).astype(f32)
    rank = jnp.sum(jnp.where(before, met, 0.0), axis=1, keepdims=True)
    return expert * PAD + rank


def slots_across(routes, k):
    before = iota((ROWS, ROWS), 0) < iota((ROWS, ROWS), 1)
    expert = routes[k : k + 1]
    met = (column(routes[0:1]) == expert).astype(f32) + (column(routes[1:2]) == expert).astype(f32)
    rank = jnp.sum(jnp.where(before, met, 0.0), axis=0, keepdims=True)
    return expert * PAD + rank


def stream_body(arrived_ref, residual_ref, routes_ref, stream_ref, outgoing_ref):
    total = residual_ref[...].astype(f32)
    projected = arrived_ref[0].astype(f32)
    for j in range(1, PEERS):
        projected = projected + arrived_ref[j].astype(f32)
    stream = (total + projected).astype(bf16)
    stream_ref[...] = stream
    routes = routes_ref[...].astype(f32)
    slot = iota((BLOCKS * PAD, ROWS), 0).astype(f32)
    placing = (slot == slots_across(routes, 0)).astype(f32) + (
        slot == slots_across(routes, 1)
    ).astype(f32)
    outgoing_ref[...] = mm(placing.astype(bf16), stream).astype(bf16)


def packed_rows(shape, packed_dim):
    packed, padded = iota(shape, packed_dim), iota(shape, 1 - packed_dim)
    block = padded // PAD
    slot = padded - block * PAD
    return ((slot < SLOTS) & (packed == block * SLOTS + slot)).astype(f32).astype(bf16)


def copies_body(arrived_ref, gain_ref, copies_ref):
    rows = mm(packed_rows((EROWS, BLOCKS * PAD), 0), arrived_ref[...]).astype(bf16)
    gain = gain_ref[...]
    high = gain.astype(bf16).astype(f32)
    middle = (gain - high).astype(bf16).astype(f32)
    low = gain - high - middle
    row = iota((16, 128), 0)
    gains = jnp.where(
        row == 0, high, jnp.where(row == 1, middle, jnp.where(row == 2, low, 0.0))
    ).astype(bf16)
    for j in range(PEERS):
        copies_ref[j, 0:EROWS, :] = rows
        copies_ref[j, EROWS:SENT, :] = gains


def expert_body(rows_ref, gate_ref, up_ref, down_ref, terms_ref, normed):
    squares = jnp.zeros((EROWS, 128), f32)
    for j in range(PEERS):
        piece = rows_ref[j, 0:EROWS, :].astype(f32)
        squares = squares + piece * piece
    mean = jnp.sum(squares, axis=1, keepdims=True) / (128 * PEERS)
    factor = lax.rsqrt(mean + epsilon)
    for j in range(PEERS):
        gains = rows_ref[j, EROWS:SENT, :].astype(f32)
        gain = gains[0:1] + gains[1:2] + gains[2:3]
        piece = rows_ref[j, 0:EROWS, :].astype(f32)
        normed[:, 128 * j : 128 * (j + 1)] = (piece * factor * gain).astype(bf16)
    rows = normed[...]
    gate = mm(rows, gate_ref[0])
    up = mm(rows, up_ref[0])
    hidden = (jax.nn.silu(gate) * up).astype(bf16)
    terms = mm(hidden, down_ref[0]).astype(bf16)
    for j in range(PEERS):
        terms_ref[j] = terms[:, 128 * j : 128 * (j + 1)]


def answer_body(terms_ref, answer_ref):
    total = terms_ref[0].astype(f32)
    for j in range(1, PEERS):
        total = total + terms_ref[j].astype(f32)
    answer_ref[...] = mm(packed_rows((BLOCKS * PAD, EROWS), 1), total.astype(bf16)).astype(bf16)


def mixture_body(returned_ref, stream_ref, routes_ref, weight_ref, out_ref):
    routes, returned = routes_ref[...].astype(f32), returned_ref[...]
    slot = iota((ROWS, BLOCKS * PAD), 1).astype(f32)
    mixture = jnp.zeros((ROWS, 128), f32)
    for k in range(2):
        pick = (slot == slots_down(routes, k)).astype(f32).astype(bf16)
        mixture = mixture + mm(pick, returned) * column(weight_ref[k : k + 1, :])
    out_ref[...] = (stream_ref[...].astype(f32) + mixture).astype(bf16)


def exchanged(pieces, axis):
    return lax.all_to_all(pieces, axis, 0, 0, tiled=True)


def shards(
    mixer_in,
    residual,
    doc_ids,
    log_step,
    log_extra,
    in_mix,
    read_mix,
    skip_gain,
    out_weight,
    norm_gain,
    routes,
    route_weight,
    switch_matrices,
    up_weight,
    down_weight,
):
    me = lax.axis_index("sp").reshape(1)
    tall = GROUPS * ROWS
    message, real, imag, keep, turn = call(
        sweep_body,
        [SMEM, SMEM, VMEM, VMEM, VMEM, VMEM],
        [
            ((BLOCKS, 16, 128), bf16),
            ((ROWS, GROUPS, 128), f32),
            ((ROWS, GROUPS, 128), f32),
            ((ROWS, GROUPS, 128), f32),
            ((2, GROUPS, 128), f32),
        ],
        [((tall, 128), f32), ((2, tall, 128), f32), ((tall, 128), f32)],
    )(me, doc_ids, log_step, log_extra.T, mixer_in, in_mix.reshape(2, 128, 128))
    messages = exchanged(message, "sp")
    (partial,) = call(
        mixer_body,
        [SMEM, SMEM] + [VMEM] * 9,
        [((PEERS, ROWS, 128), bf16)],
        [((2, tall, 128), f32), ((tall, 128), f32)],
    )(
        me, doc_ids, messages, real, imag, keep, turn,
        mixer_in, read_mix.swapaxes(2, 3).reshape(2, 128, 128), skip_gain.reshape(1, 128), out_weight,
    )
    shares = exchanged(partial, TP)
    stream, outgoing = call(
        stream_body,
        [VMEM] * 3,
        [((ROWS, 128), bf16), ((BLOCKS * PAD, 128), bf16)],
    )(shares, residual, routes.T)
    arrived = exchanged(outgoing.reshape(BLOCKS, PAD, 128), "sp").reshape(BLOCKS * PAD, 128)
    (copies,) = call(copies_body, [VMEM] * 2, [((PEERS, SENT, 128), bf16)])(
        arrived, norm_gain.reshape(1, 128)
    )
    (terms,) = call(
        expert_body,
        [VMEM] * 4,
        [((PEERS, EROWS, 128), bf16)],
        [((EROWS, 128 * PEERS), bf16)],
    )(exchanged(copies, TP), switch_matrices, up_weight, down_weight)
    (answer,) = call(answer_body, [VMEM], [((BLOCKS * PAD, 128), bf16)])(exchanged(terms, TP))
    returned = exchanged(answer.reshape(BLOCKS, PAD, 128), "sp").reshape(BLOCKS * PAD, 128)
    (out,) = call(mixture_body, [VMEM] * 4, [((ROWS, 128), bf16)])(
        returned, stream, routes.T, route_weight.T
    )
    return out


def solution(mesh):
    split = Mesh(mesh.devices.reshape(mesh.shape["sp"], 4, 4), ("sp", "tp_0", "tp_1"))
    in_specs = (
        P("sp", TP),
        P("sp", TP),
        P("sp"),
        P(None, TP),
        P("sp", TP),
        P(None, TP, None, None),
        P(None, TP, None, None),
        P(TP),
        P(TP, None),
        P(TP),
        P("sp", None),
        P("sp", None),
        P("sp", None, TP),
        P("sp", None, TP),
        P("sp", TP, None),
    )
    out_specs = P("sp", TP)
    return jax.shard_map(
        shards, mesh=split, in_specs=in_specs, out_specs=out_specs, check_vma=False
    )
```

time: 235 us -> 138 us (0.59)
  waiting for transfers between devices: 72.5 us -> 0 us
  blocking collectives: 49.3 us -> 119 us
  local copies, waits for them, and re-layouts: 39.4 us -> 0 us
  starting transfers between devices: 39 us -> 0 us
  Pallas kernels: 0 us -> 17.4 us
  other arithmetic: 15.7 us -> 0 us
  between operations: 11.3 us -> 0.01 us
  matrix products: 4.14 us -> 0 us
  loops' own time: 2.91 us -> 0 us
    all_to_all x2 -> x6, blocking collectives: 35.9 us -> 119 us  [exchanged(): return lax.all_to_all(pieces, axis, 0, 0, tiled=True)]
    all_to_all x5 -> x0, waiting for transfers between devices: 72.5 us -> none  [the longest x2 41.9 us: copy_for_each(): lax.all_to_all(jnp.broadcast_to(shard[None], (devices, *shard.shape)), ax...]
    all_to_all x5 -> x0, starting transfers between devices: 39 us -> none  [the longest x2 20.8 us: copy_for_each(): lax.all_to_all(jnp.broadcast_to(shard[None], (devices, *shard.shape)), ax...]
    pallas_call x0 -> x7, Pallas kernels: none -> 17.4 us  [the longest x1 3.87 us: shards(): call(expert_body, [VMEM] * 4, [((PEERS, EROWS, 128), bf16)], [((EROWS, 12...]
    psum x2 -> x0, blocking collectives: 13.4 us -> none  [by_axis(): return functools.reduce(lax.psum, axes, shard)]
    slice x125 -> x0, local copies, waits for them, and re-layouts: 11 us -> none  [the longest x114 9.05 us: folded_in_pairs(): part[side::2]]
    dynamic_update_slice x128 -> x0, local copies, waits for them, and re-layouts: 8.02 us -> none  [run_chain(): lax.scan(across, (unit_state, empty_state, empty_state, empty_state), lan...]
    reshape x24 -> x0, local copies, waits for them, and re-layouts: 5.75 us -> none  [the longest x16 3.59 us: spread_back(): return jnp.swapaxes(member, 0, 1).reshape(row_count, state_width)]
  transfers between devices with their start and end apart: 5 -> 0, of which waited for: 5 -> 0; matrix products, arithmetic and copies ran while one was open for 9% -> 0% of each run, Pallas kernels for 0% -> 0%
where the time goes in v1:
time: 138 us; the launch traced here: 137 us
  blocking collectives  119 us (86%)
  Pallas kernels  17.4 us (13%)
    all_to_all x6, blocking collectives, exchanged(): return lax.all_to_all(pieces, axis, 0, 0, tiled=True)  119 us
    pallas_call x1, Pallas kernels, shards(): call(expert_body, [VMEM] * 4, [((PEERS, EROWS, 128), bf16)], [((EROWS, 12...  3.87 us
    pallas_call x1, Pallas kernels, shards(): call(mixer_body, [SMEM, SMEM] + [VMEM] * 9, [((PEERS, ROWS, 128), bf16)],...  3.23 us
    pallas_call x1, Pallas kernels, shards(): call(sweep_body, [SMEM, SMEM, VMEM, VMEM, VMEM, VMEM], [((BLOCKS, 16, 128...  2.82 us

profile of v1, /device:TPU:1, one launch (start us, length us, event | category | flops | bytes accessed | tf_op | source)
XLA Modules:
  0.0 136.8 jit_solution(5561844690617238696)
XLA Ops:
  0.0 2.8 %shard_map.145 = (bf16[32,16,128]{2,1,0:T(8,128)(2,1)}, f32[64,8,128]{2,1,0:T(8,128)}, f32[64,8,128]{2,1,0:T(8,128)}, f32[64,8,128]{2,1,0:T(8,128)}, f32[2,8,128]{2,1,0:T(8,128)}) custom-call(s32[1]{0:T(128)} %bitcast.me_ref, s32[64]{0:T(128)} %docs_ref.3, f32[2,8]{1,0:T(2,128)} %log_step_ref.1, f32[8,64]{1,0:T(8,128)} %bitcast.22, bf16[64,128]{1,0:T(8,128)(2,1)} %x_ref.3, ...), custom_call_target="tpu_custom_call" | custom-call | tf_op jit(solution)/shard_map/pallas_call | solution.py:334
  2.8 32.7 %all_to_all.30.message_ref = bf16[32,16,128]{2,1,0:T(8,128)(2,1)} all-to-all(bf16[32,16,128]{2,1,0:T(8,128)(2,1)} %get-tuple-element.12), channel_id=1, replica_groups=mesh['sp'=32,'tp_0'=4,'tp_1'=4] {'sp'}, dimensions={0} | all-to-all | bytes 262144 | tf_op jit(solution)/shard_map/all_to_all | solution.py:312
  35.5 3.2 %shard_map.146 = bf16[16,64,128]{2,1,0:T(8,128)(2,1)} custom-call(s32[1]{0:T(128)} %bitcast.me_ref, s32[64]{0:T(128)} %docs_ref.3, bf16[32,16,128]{2,1,0:T(8,128)(2,1)} %all_to_all.30.message_ref, f32[64,8,128]{2,1,0:T(8,128)} %get-tuple-element.13.real_ref, f32[64,8,128]{2,1,0:T(8,128)} %get-tuple-element.14.imag_ref, ...), custom_call_target="tpu_custom_call" | custom-call | tf_op jit(solution)/shard_map/pallas_call | solution.py:347
  38.7 14.5 %all_to_all.31.arrived_ref = bf16[16,64,128]{2,1,0:T(8,128)(2,1)} all-to-all(bf16[16,64,128]{2,1,0:T(8,128)(2,1)} %shard_map.146), channel_id=1, replica_groups=mesh['sp'=32,'tp_0'=4,'tp_1'=4] {'tp_0','tp_1'}, dimensions={0} | all-to-all | bytes 524288 | tf_op jit(solution)/shard_map/all_to_all | solution.py:312
  53.2 1.9 %shard_map.147 = (bf16[64,128]{1,0:T(8,128)(2,1)}, bf16[256,128]{1,0:T(8,128)(2,1)}) custom-call(bf16[16,64,128]{2,1,0:T(8,128)(2,1)} %all_to_all.31.arrived_ref, bf16[64,128]{1,0:T(8,128)(2,1)} %residual_ref.1, s32[2,64]{1,0:T(2,128)} %bitcast.20), custom_call_target="tpu_custom_call" | custom-call | tf_op jit(solution)/shard_map/pallas_call | solution.py:357
  55.1 20.1 %all_to_all.32 = bf16[32,8,128]{2,1,0:T(8,128)(2,1)} all-to-all(bf16[32,8,128]{2,1,0:T(8,128)(2,1)} %bitcast.19), channel_id=1, replica_groups=mesh['sp'=32,'tp_0'=4,'tp_1'=4] {'sp'}, dimensions={0} | all-to-all | bytes 131072 | tf_op jit(solution)/shard_map/all_to_all | solution.py:312
  75.2 1.9 %shard_map.148 = bf16[16,176,128]{2,1,0:T(8,128)(2,1)} custom-call(bf16[256,128]{1,0:T(8,128)(2,1)} %bitcast.15, f32[1,128]{1,0:T(1,128)} %bitcast.24), custom_call_target="tpu_custom_call" | custom-call | tf_op jit(solution)/shard_map/pallas_call | solution.py:363
  77.1 16.1 %all_to_all.33.rows_ref = bf16[16,176,128]{2,1,0:T(8,128)(2,1)} all-to-all(bf16[16,176,128]{2,1,0:T(8,128)(2,1)} %shard_map.148), channel_id=1, replica_groups=mesh['sp'=32,'tp_0'=4,'tp_1'=4] {'tp_0','tp_1'}, dimensions={0} | all-to-all | bytes 1441792 | tf_op jit(solution)/shard_map/all_to_all | solution.py:312
  93.2 3.9 %shard_map.149 = bf16[16,160,128]{2,1,0:T(8,128)(2,1)} custom-call(bf16[16,176,128]{2,1,0:T(8,128)(2,1)} %all_to_all.33.rows_ref, bf16[1,2048,256]{2,1,0:T(8,128)(2,1)} %gate_ref.1, bf16[1,2048,256]{2,1,0:T(8,128)(2,1)} %up_ref.1, bf16[1,256,2048]{2,1,0:T(8,128)(2,1)} %down_ref.1), custom_call_target="tpu_custom_call" | custom-call | tf_op jit(solution)/shard_map/pallas_call | solution.py:366
  97.1 14.6 %all_to_all.34.terms_ref = bf16[16,160,128]{2,1,0:T(8,128)(2,1)} all-to-all(bf16[16,160,128]{2,1,0:T(8,128)(2,1)} %shard_map.149), channel_id=1, replica_groups=mesh['sp'=32,'tp_0'=4,'tp_1'=4] {'tp_0','tp_1'}, dimensions={0} | all-to-all | bytes 1310720 | tf_op jit(solution)/shard_map/all_to_all | solution.py:312
  111.7 2.0 %shard_map.150 = bf16[256,128]{1,0:T(8,128)(2,1)} custom-call(bf16[16,160,128]{2,1,0:T(8,128)(2,1)} %all_to_all.34.terms_ref), custom_call_target="tpu_custom_call" | custom-call | tf_op jit(solution)/shard_map/pallas_call | solution.py:372
  113.7 21.4 %all_to_all.35 = bf16[32,8,128]{2,1,0:T(8,128)(2,1)} all-to-all(bf16[32,8,128]{2,1,0:T(8,128)(2,1)} %bitcast.16), channel_id=1, replica_groups=mesh['sp'=32,'tp_0'=4,'tp_1'=4] {'sp'}, dimensions={0} | all-to-all | bytes 131072 | tf_op jit(solution)/shard_map/all_to_all | solution.py:312
  135.1 1.8 %shard_map.151 = bf16[64,128]{1,0:T(8,128)(2,1)} custom-call(bf16[256,128]{1,0:T(8,128)(2,1)} %bitcast.14, bf16[64,128]{1,0:T(8,128)(2,1)} %get-tuple-element.18.stream_ref, s32[2,64]{1,0:T(2,128)} %bitcast.21, f32[2,64]{1,0:T(2,128)} %bitcast.23), custom_call_target="tpu_custom_call" | custom-call | tf_op jit(solution)/shard_map/pallas_call | solution.py:374

commit v2 on v1

--- a/solution.py
+++ b/solution.py
@@ -26,13 +26,19 @@
 SMEM = pl.BlockSpec(memory_space=pltpu.SMEM)
 
 
-def call(body, in_specs, outs, scratch=()):
+def near(x):
+    return x if INTERPRET else pltpu.with_memory_space_constraint(x, pltpu.VMEM)
+
+
+def call(body, in_specs, outs, scratch=(), last=False):
+    kept = jax.ShapeDtypeStruct if INTERPRET or last else pltpu.VMEM
     return pl.pallas_call(
         body,
         in_specs=in_specs,
         out_specs=[VMEM] * len(outs),
-        out_shape=[jax.ShapeDtypeStruct(shape, dtype) for shape, dtype in outs],
+        out_shape=[kept(shape, dtype) for shape, dtype in outs],
         scratch_shapes=[pltpu.VMEM(shape, dtype) for shape, dtype in scratch],
+        compiler_params=pltpu.CompilerParams(vmem_limit_bytes=16 * 2**20),
         interpret=INTERPRET,
     )
 
@@ -343,17 +349,18 @@
         ],
         [((tall, 128), f32), ((2, tall, 128), f32), ((tall, 128), f32)],
     )(me, doc_ids, log_step, log_extra.T, mixer_in, in_mix.reshape(2, 128, 128))
-    messages = exchanged(message, "sp")
+    messages = near(exchanged(message, "sp"))
     (partial,) = call(
         mixer_body,
         [SMEM, SMEM] + [VMEM] * 9,
         [((PEERS, ROWS, 128), bf16)],
         [((2, tall, 128), f32), ((tall, 128), f32)],
     )(
-        me, doc_ids, messages, real, imag, keep, turn,
-        mixer_in, read_mix.swapaxes(2, 3).reshape(2, 128, 128), skip_gain.reshape(1, 128), out_weight,
-    )
-    shares = exchanged(partial, TP)
+        me, doc_ids, messages, near(real), near(imag), near(keep), near(turn), mixer_in,
+        read_mix.swapaxes(2, 3).reshape(2, 128, 128), skip_gain.reshape(1, 128),
+        out_weight,
+    )
+    shares = near(exchanged(partial, TP))
     stream, outgoing = call(
         stream_body,
         [VMEM] * 3,
@@ -361,18 +368,20 @@
     )(shares, residual, routes.T)
     arrived = exchanged(outgoing.reshape(BLOCKS, PAD, 128), "sp").reshape(BLOCKS * PAD, 128)
     (copies,) = call(copies_body, [VMEM] * 2, [((PEERS, SENT, 128), bf16)])(
-        arrived, norm_gain.reshape(1, 128)
+        near(arrived), norm_gain.reshape(1, 128)
     )
     (terms,) = call(
         expert_body,
         [VMEM] * 4,
         [((PEERS, EROWS, 128), bf16)],
         [((EROWS, 128 * PEERS), bf16)],
-    )(exchanged(copies, TP), switch_matrices, up_weight, down_weight)
-    (answer,) = call(answer_body, [VMEM], [((BLOCKS * PAD, 128), bf16)])(exchanged(terms, TP))
+    )(near(exchanged(copies, TP)), switch_matrices, up_weight, down_weight)
+    (answer,) = call(answer_body, [VMEM], [((BLOCKS * PAD, 128), bf16)])(
+        near(exchanged(terms, TP))
+    )
     returned = exchanged(answer.reshape(BLOCKS, PAD, 128), "sp").reshape(BLOCKS * PAD, 128)
-    (out,) = call(mixture_body, [VMEM] * 4, [((ROWS, 128), bf16)])(
-        returned, stream, routes.T, route_weight.T
+    (out,) = call(mixture_body, [VMEM] * 4, [((ROWS, 128), bf16)], last=True)(
+        near(returned), near(stream), routes.T, route_weight.T
     )
     return out
 

time: 138 us -> 125 us (0.906)
  Pallas kernels: 17.4 us -> 5.77 us
  blocking collectives: 119 us -> 114 us
  local copies, waits for them, and re-layouts: 0 us -> 4.73 us
    all_to_all x6, blocking collectives: 119 us -> 114 us  [exchanged(): return lax.all_to_all(pieces, axis, 0, 0, tiled=True)]
    unnamed x0 -> x30, local copies, waits for them, and re-layouts: none -> 4.73 us
    pallas_call x1, Pallas kernels: 3.87 us -> 0.94 us  [shards(): call(expert_body, [VMEM] * 4, [((PEERS, EROWS, 128), bf16)], [((EROWS, 12...]
    pallas_call x1, Pallas kernels: 1.96 us -> 0.26 us  [shards(): call(answer_body, [VMEM], [((BLOCKS * PAD, 128), bf16)])]
    pallas_call x1, Pallas kernels: 1.89 us -> 0.18 us  [shards(): call(copies_body, [VMEM] * 2, [((PEERS, SENT, 128), bf16)])]
    pallas_call x1, Pallas kernels: 1.86 us -> 0.25 us  [shards(): call(stream_body, [VMEM] * 3, [((ROWS, 128), bf16), ((BLOCKS * PAD, 128),...]
    pallas_call x1, Pallas kernels: 3.23 us -> 1.64 us  [shards(): call(mixer_body, [SMEM, SMEM] + [VMEM] * 9, [((PEERS, ROWS, 128), bf16)],...]
where the time goes in v2:
time: 125 us
  blocking collectives  114 us (91%)
  Pallas kernels  5.77 us (5%)
  local copies, waits for them, and re-layouts  4.73 us (4%)
    all_to_all x6, blocking collectives, exchanged(): return lax.all_to_all(pieces, axis, 0, 0, tiled=True)  114 us
    unnamed x30, local copies, waits for them, and re-layouts  4.73 us

profile of v2, /device:TPU:1, one launch (start us, length us, event | category | flops | bytes accessed | tf_op | source)
XLA Modules:
  0.0 125.0 jit_solution(15639566040477597292)
XLA Ops:
  0.0 0.0 copy-start.9
  0.0 0.0 copy-start.10
  0.0 0.0 copy-start.11
  0.0 0.7 copy-done.9
  0.7 0.0 copy-done.10
  0.7 0.0 copy-done.11
  0.7 0.0 copy-start.5
  0.7 0.9 copy-done.5
  1.6 0.0 copy-start.6
  1.6 0.7 copy-done.6
  2.3 1.6 %shard_map.145 = (bf16[32,16,128]{2,1,0:T(8,128)(2,1)S(1)}, f32[64,8,128]{2,1,0:T(8,128)S(1)}, f32[64,8,128]{2,1,0:T(8,128)S(1)}, f32[64,8,128]{2,1,0:T(8,128)S(1)}, f32[2,8,128]{2,1,0:T(8,128)S(1)}) custom-call(s32[1]{0:T(128)} %bitcast.me_ref, s32[64]{0:T(128)S(1)} %copy-done.10, f32[2,8]{1,0:T(2,128)S(1)} %copy-done.11, f32[8,64]{1,0:T(8,128)S(1)} %bitcast.22, ...), custom_call_target="tpu_custom_call" | custom-call | tf_op jit(solution)/shard_map/pallas_call | solution.py:340
  3.9 0.0 copy-start.4
  3.9 32.5 %all_to_all.30.message_ref = bf16[32,16,128]{2,1,0:T(8,128)(2,1)S(1)} all-to-all(bf16[32,16,128]{2,1,0:T(8,128)(2,1)S(1)} %get-tuple-element.12), channel_id=1, replica_groups=mesh['sp'=32,'tp_0'=4,'tp_1'=4] {'sp'}, dimensions={0} | all-to-all | bytes 262144 | tf_op jit(solution)/shard_map/all_to_all | solution.py:318
  36.5 0.0 copy-start.14
  36.5 0.0 copy-done.4
  36.5 0.7 copy-done.14
  37.1 0.0 copy-start.3
  37.1 1.0 copy-done.3
  38.2 0.0 copy-start.7
  38.2 0.0 copy-start.8
  38.2 0.0 copy-start.13
  38.2 1.6 %shard_map.146 = bf16[16,64,128]{2,1,0:T(8,128)(2,1)S(1)} custom-call(s32[1]{0:T(128)} %bitcast.me_ref, s32[64]{0:T(128)S(1)} %copy-done.10, bf16[32,16,128]{2,1,0:T(8,128)(2,1)S(1)} %all_to_all.30.message_ref, f32[64,8,128]{2,1,0:T(8,128)S(1)} %get-tuple-element.13.real_ref, f32[64,8,128]{2,1,0:T(8,128)S(1)} %get-tuple-element.14.imag_ref, ...), custom_call_target="tpu_custom_call" | custom-call | tf_op jit(solution)/shard_map/pallas_call | solution.py:353
  39.8 0.0 copy-start.2
  39.8 14.3 %all_to_all.31.arrived_ref = bf16[16,64,128]{2,1,0:T(8,128)(2,1)S(1)} all-to-all(bf16[16,64,128]{2,1,0:T(8,128)(2,1)S(1)} %shard_map.146), channel_id=1, replica_groups=mesh['sp'=32,'tp_0'=4,'tp_1'=4] {'tp_0','tp_1'}, dimensions={0} | all-to-all | bytes 524288 | tf_op jit(solution)/shard_map/all_to_all | solution.py:318
  54.1 0.0 copy-done.7
  54.1 0.0 copy-done.8
  54.1 0.3 shard_map.147
  54.4 18.6 %all_to_all.32 = bf16[32,8,128]{2,1,0:T(8,128)(2,1)S(1)} all-to-all(bf16[32,8,128]{2,1,0:T(8,128)(2,1)S(1)} %bitcast.19), channel_id=1, replica_groups=mesh['sp'=32,'tp_0'=4,'tp_1'=4] {'sp'}, dimensions={0} | all-to-all | bytes 131072 | tf_op jit(solution)/shard_map/all_to_all | solution.py:318
  73.0 0.0 copy-done.13
  73.0 0.0 copy-start
  73.0 0.0 copy-start.1
  73.0 0.2 shard_map.148
  73.2 14.6 %all_to_all.33.rows_ref = bf16[16,176,128]{2,1,0:T(8,128)(2,1)S(1)} all-to-all(bf16[16,176,128]{2,1,0:T(8,128)(2,1)S(1)} %shard_map.148), channel_id=1, replica_groups=mesh['sp'=32,'tp_0'=4,'tp_1'=4] {'tp_0','tp_1'}, dimensions={0} | all-to-all | bytes 1441792 | tf_op jit(solution)/shard_map/all_to_all | solution.py:318
  87.8 0.0 copy-done.2
  87.8 0.0 copy-done
  87.8 0.0 copy-done.1
  87.8 0.9 shard_map.149
  88.8 13.1 %all_to_all.34.terms_ref = bf16[16,160,128]{2,1,0:T(8,128)(2,1)S(1)} all-to-all(bf16[16,160,128]{2,1,0:T(8,128)(2,1)S(1)} %shard_map.149), channel_id=1, replica_groups=mesh['sp'=32,'tp_0'=4,'tp_1'=4] {'tp_0','tp_1'}, dimensions={0} | all-to-all | bytes 1310720 | tf_op jit(solution)/shard_map/all_to_all | solution.py:318
  101.8 0.3 shard_map.150
  102.1 21.3 %all_to_all.35 = bf16[32,8,128]{2,1,0:T(8,128)(2,1)S(1)} all-to-all(bf16[32,8,128]{2,1,0:T(8,128)(2,1)S(1)} %bitcast.16), channel_id=1, replica_groups=mesh['sp'=32,'tp_0'=4,'tp_1'=4] {'sp'}, dimensions={0} | all-to-all | bytes 131072 | tf_op jit(solution)/shard_map/all_to_all | solution.py:318
  123.4 0.0 copy-start.12
  123.4 0.7 copy-done.12
  124.1 0.9 shard_map.151
Async XLA Ops:
  0.0 0.7 copy-start.9
  0.0 0.7 copy-start.10
  0.0 0.7 copy-start.11
  0.7 0.9 copy-start.5
  1.6 0.7 copy-start.6
  3.9 32.5 %copy-start.4 = (f32[2,8,128,16]{2,3,1,0:T(8,128)S(1)}, f32[2,8,128,16]{2,3,1,0:T(8,128)}, u32[]{:S(2)}) copy-start(f32[2,8,128,16]{2,3,1,0:T(8,128)} %param.21) | copy-start | bytes 393220
  36.5 0.7 copy-start.14
  37.1 1.0 copy-start.3
  38.2 16.0 %copy-start.7 = (bf16[64,128]{1,0:T(8,128)(2,1)S(1)}, bf16[64,128]{1,0:T(8,128)(2,1)}, u32[]{:S(2)}) copy-start(bf16[64,128]{1,0:T(8,128)(2,1)} %residual_ref.1) | copy-start | bytes 49156
  38.2 16.0 %copy-start.8 = (s32[64,2]{0,1:T(2,128)S(1)}, s32[64,2]{0,1:T(2,128)}, u32[]{:S(2)}) copy-start(s32[64,2]{0,1:T(2,128)} %param.25) | copy-start | bytes 1540
  38.2 34.8 %copy-start.13 = (f32[128]{0:T(128)S(1)}, f32[128]{0:T(128)}, u32[]{:S(2)}) copy-start(f32[128]{0:T(128)} %param.24) | copy-start | bytes 1540
  39.8 48.0 %copy-start.2 = (bf16[1,256,2048]{2,1,0:T(8,128)(2,1)S(1)}, bf16[1,256,2048]{2,1,0:T(8,128)(2,1)}, u32[]{:S(2)}) copy-start(bf16[1,256,2048]{2,1,0:T(8,128)(2,1)} %down_ref.1) | copy-start | bytes 3145732
  73.0 14.8 %copy-start = (bf16[1,2048,256]{2,1,0:T(8,128)(2,1)S(1)}, bf16[1,2048,256]{2,1,0:T(8,128)(2,1)}, u32[]{:S(2)}) copy-start(bf16[1,2048,256]{2,1,0:T(8,128)(2,1)} %gate_ref.1) | copy-start | bytes 3145732
  73.0 14.8 %copy-start.1 = (bf16[1,2048,256]{2,1,0:T(8,128)(2,1)S(1)}, bf16[1,2048,256]{2,1,0:T(8,128)(2,1)}, u32[]{:S(2)}) copy-start(bf16[1,2048,256]{2,1,0:T(8,128)(2,1)} %up_ref.1) | copy-start | bytes 3145732
  123.4 0.7 copy-start.12

commit v3 on v2

--- a/solution.py
+++ b/solution.py
@@ -24,20 +24,29 @@
 
 VMEM = pl.BlockSpec(memory_space=pltpu.VMEM)
 SMEM = pl.BlockSpec(memory_space=pltpu.SMEM)
+FAR = pl.BlockSpec(memory_space=pl.ANY if INTERPRET else pltpu.HBM)
 
 
 def near(x):
     return x if INTERPRET else pltpu.with_memory_space_constraint(x, pltpu.VMEM)
 
 
-def call(body, in_specs, outs, scratch=(), last=False):
+def far(x):
+    return x if INTERPRET else pltpu.with_memory_space_constraint(x, pltpu.HBM)
+
+
+def call(body, in_specs, outs, scratch=(), copies=0, last=False):
     kept = jax.ShapeDtypeStruct if INTERPRET or last else pltpu.VMEM
     return pl.pallas_call(
         body,
         in_specs=in_specs,
         out_specs=[VMEM] * len(outs),
         out_shape=[kept(shape, dtype) for shape, dtype in outs],
-        scratch_shapes=[pltpu.VMEM(shape, dtype) for shape, dtype in scratch],
+        scratch_shapes=[
+            (pltpu.SMEM if dtype == jnp.int32 else pltpu.VMEM)(shape, dtype)
+            for shape, dtype in scratch
+        ]
+        + ([pltpu.SemaphoreType.DMA((copies,))] if copies else []),
         compiler_params=pltpu.CompilerParams(vmem_limit_bytes=16 * 2**20),
         interpret=INTERPRET,
     )
@@ -85,10 +94,26 @@
 
 
 def sweep_body(
-    me_ref, docs_ref, log_step_ref, log_extra_ref, x_ref, in_mix_ref,
+    me_ref, far_docs, far_step, far_extra, far_x, far_mix,
     message_ref, real_ref, imag_ref, keep_ref, turn_ref,
-    masked, source, magnitude,
+    masked, source, magnitude, log_step_ref, log_extra_ref, x_ref, in_mix_ref, docs_ref, arrivals,
 ):
+    here_now = [
+        pltpu.make_async_copy(far, near_ref, arrivals.at[k])
+        for k, (far, near_ref) in enumerate(
+            [
+                (far_mix, in_mix_ref),
+                (far_x, x_ref),
+                (far_extra, log_extra_ref),
+                (far_step, log_step_ref),
+                (far_docs, docs_ref),
+            ]
+        )
+    ]
+    for copy in here_now:
+        copy.start()
+    for copy in here_now[::-1]:
+        copy.wait()
     lane = iota((GROUPS, 128), 1)
     fwd = lane < 64
     step = steps_by_lane(log_step_ref[...])
@@ -137,6 +162,7 @@
     decay = jnp.where((lane & 32) == 0, high, crossed - high)
     first_doc = docs_ref[0].astype(f32)
     last_doc = docs_ref[ROWS - 1].astype(f32)
+    turn_ref[2] = jnp.where(fwd, first_doc, last_doc)
     to_later = jnp.concatenate(
         [jnp.where(fwd, real, decay), jnp.where(fwd, imag, last_doc)], axis=0
     ).astype(bf16)
@@ -155,17 +181,24 @@
 
 
 def mixer_body(
-    me_ref, docs_ref, message_ref, real_ref, imag_ref, keep_ref, turn_ref,
-    x_ref, read_mix_ref, skip_ref, out_weight_ref,
+    me_ref, message_ref, real_ref, imag_ref, keep_ref, turn_ref,
+    far_x, far_read, far_skip, far_weight,
     partial_ref,
-    states, read_out,
+    states, read_out, x_ref, read_mix_ref, skip_ref, out_weight_ref, arrivals,
 ):
+    here_now = [
+        pltpu.make_async_copy(far, near_ref, arrivals.at[k])
+        for k, (far, near_ref) in enumerate(
+            [(far_read, read_mix_ref), (far_x, x_ref), (far_skip, skip_ref), (far_weight, out_weight_ref)]
+        )
+    ]
+    for copy in here_now:
+        copy.start()
     lane = iota((GROUPS, 128), 1)
     fwd = lane < 64
     odd = (lane & 32) != 0
     me = me_ref[0]
-    mine = jnp.where(fwd, docs_ref[0].astype(f32), docs_ref[ROWS - 1].astype(f32))
-    cos, sin = turn_ref[0], turn_ref[1]
+    cos, sin, mine = turn_ref[0], turn_ref[1], turn_ref[2]
     block_cos, block_sin = cos, sin
     for _ in range(6):
         block_cos, block_sin = (
@@ -202,6 +235,8 @@
         states[0, there, 64:128] = real[:, 64:128]
         states[1, here, 0:64] = imag[:, 0:64]
         states[1, there, 64:128] = imag[:, 64:128]
+    for copy in here_now:
+        copy.wait()
     read_real, read_imag = halves_joined(read_mix_ref[0], read_mix_ref[1])
     read_out[...] = mm_across(states[0].astype(bf16), read_real.astype(bf16)) + mm_across(
         states[1].astype(bf16), read_imag.astype(bf16)
@@ -239,7 +274,10 @@
     return expert * PAD + rank
 
 
-def stream_body(arrived_ref, residual_ref, routes_ref, stream_ref, outgoing_ref):
+def stream_body(
+    arrived_ref, residual_ref, routes_ref, weight_ref, stream_ref, outgoing_ref, weights_ref
+):
+    weights_ref[...] = weight_ref[...]
     total = residual_ref[...].astype(f32)
     projected = arrived_ref[0].astype(f32)
     for j in range(1, PEERS):
@@ -339,33 +377,53 @@
     tall = GROUPS * ROWS
     message, real, imag, keep, turn = call(
         sweep_body,
-        [SMEM, SMEM, VMEM, VMEM, VMEM, VMEM],
+        [SMEM, FAR, FAR, FAR, FAR, FAR],
         [
             ((BLOCKS, 16, 128), bf16),
             ((ROWS, GROUPS, 128), f32),
             ((ROWS, GROUPS, 128), f32),
             ((ROWS, GROUPS, 128), f32),
-            ((2, GROUPS, 128), f32),
+            ((3, GROUPS, 128), f32),
         ],
-        [((tall, 128), f32), ((2, tall, 128), f32), ((tall, 128), f32)],
-    )(me, doc_ids, log_step, log_extra.T, mixer_in, in_mix.reshape(2, 128, 128))
+        [
+            ((tall, 128), f32),
+            ((2, tall, 128), f32),
+            ((tall, 128), f32),
+            ((2, GROUPS), f32),
+            ((GROUPS, ROWS), f32),
+            ((ROWS, 128), bf16),
+            ((2, 128, 128), f32),
+            ((ROWS,), jnp.int32),
+        ],
+        copies=5,
+    )(
+        me, far(doc_ids), far(log_step), far(log_extra.T), far(mixer_in), far(in_mix.reshape(2, 128, 128))
+    )
     messages = near(exchanged(message, "sp"))
     (partial,) = call(
         mixer_body,
-        [SMEM, SMEM] + [VMEM] * 9,
+        [SMEM] + [VMEM] * 5 + [FAR] * 4,
         [((PEERS, ROWS, 128), bf16)],
-        [((2, tall, 128), f32), ((tall, 128), f32)],
+        [
+            ((2, tall, 128), f32),
+            ((tall, 128), f32),
+            ((ROWS, 128), bf16),
+            ((2, 128, 128), f32),
+            ((1, 128), f32),
+            ((128, 128 * PEERS), bf16),
+        ],
+        copies=4,
     )(
-        me, doc_ids, messages, near(real), near(imag), near(keep), near(turn), mixer_in,
-        read_mix.swapaxes(2, 3).reshape(2, 128, 128), skip_gain.reshape(1, 128),
-        out_weight,
+        me, messages, near(real), near(imag), near(keep), near(turn), far(mixer_in),
+        far(read_mix.swapaxes(2, 3).reshape(2, 128, 128)), far(skip_gain.reshape(1, 128)),
+        far(out_weight),
     )
     shares = near(exchanged(partial, TP))
-    stream, outgoing = call(
+    stream, outgoing, weights = call(
         stream_body,
-        [VMEM] * 3,
-        [((ROWS, 128), bf16), ((BLOCKS * PAD, 128), bf16)],
-    )(shares, residual, routes.T)
+        [VMEM] * 4,
+        [((ROWS, 128), bf16), ((BLOCKS * PAD, 128), bf16), ((2, ROWS), f32)],
+    )(shares, residual, routes.T, route_weight.T)
     arrived = exchanged(outgoing.reshape(BLOCKS, PAD, 128), "sp").reshape(BLOCKS * PAD, 128)
     (copies,) = call(copies_body, [VMEM] * 2, [((PEERS, SENT, 128), bf16)])(
         near(arrived), norm_gain.reshape(1, 128)
@@ -381,7 +439,7 @@
     )
     returned = exchanged(answer.reshape(BLOCKS, PAD, 128), "sp").reshape(BLOCKS * PAD, 128)
     (out,) = call(mixture_body, [VMEM] * 4, [((ROWS, 128), bf16)], last=True)(
-        near(returned), near(stream), routes.T, route_weight.T
+        near(returned), near(stream), routes.T, near(weights)
     )
     return out
 

time: 125 us -> 121 us (0.968)
  local copies, waits for them, and re-layouts: 4.73 us -> 0.03 us
    unnamed x30 -> x14, local copies, waits for them, and re-layouts: 4.73 us -> 0.03 us
where the time goes in v3:
time: 121 us
  blocking collectives  114 us (94%)
  Pallas kernels  6.63 us (5%)
    all_to_all x6, blocking collectives, exchanged(): return lax.all_to_all(pieces, axis, 0, 0, tiled=True)  114 us

profile of v3, /device:TPU:1, one launch (start us, length us, event | category | flops | bytes accessed | tf_op | source)
XLA Modules:
  0.0 121.0 jit_solution(8087217456192513484)
XLA Ops:
  0.0 2.0 %shard_map.145 = (bf16[32,16,128]{2,1,0:T(8,128)(2,1)S(1)}, f32[64,8,128]{2,1,0:T(8,128)S(1)}, f32[64,8,128]{2,1,0:T(8,128)S(1)}, f32[64,8,128]{2,1,0:T(8,128)S(1)}, f32[3,8,128]{2,1,0:T(8,128)S(1)}) custom-call(s32[1]{0:T(128)} %bitcast.me_ref, s32[64]{0:T(128)} %far_docs.1, f32[2,8]{1,0:T(2,128)} %far_step.1, f32[8,64]{1,0:T(8,128)} %bitcast.24, ...), custom_call_target="tpu_custom_call" | custom-call | tf_op jit(solution)/shard_map/pallas_call | solution.py:378
  2.0 32.4 %all_to_all.30.message_ref = bf16[32,16,128]{2,1,0:T(8,128)(2,1)S(1)} all-to-all(bf16[32,16,128]{2,1,0:T(8,128)(2,1)S(1)} %get-tuple-element.13), channel_id=1, replica_groups=mesh['sp'=32,'tp_0'=4,'tp_1'=4] {'sp'}, dimensions={0} | all-to-all | bytes 262144 | tf_op jit(solution)/shard_map/all_to_all | solution.py:356
  34.4 0.0 copy-start.3
  34.4 0.0 copy-start.4
  34.4 0.0 copy-start.5
  34.4 0.0 copy-start.6
  34.4 2.1 %shard_map.146 = bf16[16,64,128]{2,1,0:T(8,128)(2,1)S(1)} custom-call(s32[1]{0:T(128)} %bitcast.me_ref, bf16[32,16,128]{2,1,0:T(8,128)(2,1)S(1)} %all_to_all.30.message_ref, f32[64,8,128]{2,1,0:T(8,128)S(1)} %get-tuple-element.14.real_ref, f32[64,8,128]{2,1,0:T(8,128)S(1)} %get-tuple-element.15.imag_ref, f32[64,8,128]{2,1,0:T(8,128)S(1)} %get-tuple-element.16.keep_ref, ...), custom_call_target="tpu_custom_call" | custom-call | tf_op jit(solution)/shard_map/pallas_call | solution.py:403
  36.5 0.0 copy-start.2
  36.5 14.3 %all_to_all.31.arrived_ref = bf16[16,64,128]{2,1,0:T(8,128)(2,1)S(1)} all-to-all(bf16[16,64,128]{2,1,0:T(8,128)(2,1)S(1)} %shard_map.146), channel_id=1, replica_groups=mesh['sp'=32,'tp_0'=4,'tp_1'=4] {'tp_0','tp_1'}, dimensions={0} | all-to-all | bytes 524288 | tf_op jit(solution)/shard_map/all_to_all | solution.py:356
  50.8 0.0 copy-done.3
  50.8 0.0 copy-done.4
  50.8 0.0 copy-done.5
  50.8 0.3 shard_map.147
  51.1 18.6 %all_to_all.32 = bf16[32,8,128]{2,1,0:T(8,128)(2,1)S(1)} all-to-all(bf16[32,8,128]{2,1,0:T(8,128)(2,1)S(1)} %bitcast.17), channel_id=1, replica_groups=mesh['sp'=32,'tp_0'=4,'tp_1'=4] {'sp'}, dimensions={0} | all-to-all | bytes 131072 | tf_op jit(solution)/shard_map/all_to_all | solution.py:356
  69.6 0.0 copy-done.6
  69.6 0.0 copy-start
  69.7 0.0 copy-start.1
  69.7 0.2 shard_map.148
  69.8 14.6 %all_to_all.33.rows_ref = bf16[16,176,128]{2,1,0:T(8,128)(2,1)S(1)} all-to-all(bf16[16,176,128]{2,1,0:T(8,128)(2,1)S(1)} %shard_map.148), channel_id=1, replica_groups=mesh['sp'=32,'tp_0'=4,'tp_1'=4] {'tp_0','tp_1'}, dimensions={0} | all-to-all | bytes 1441792 | tf_op jit(solution)/shard_map/all_to_all | solution.py:356
  84.5 0.0 copy-done.2
  84.5 0.0 copy-done
  84.5 0.0 copy-done.1
  84.5 0.9 shard_map.149
  85.5 13.1 %all_to_all.34.terms_ref = bf16[16,160,128]{2,1,0:T(8,128)(2,1)S(1)} all-to-all(bf16[16,160,128]{2,1,0:T(8,128)(2,1)S(1)} %shard_map.149), channel_id=1, replica_groups=mesh['sp'=32,'tp_0'=4,'tp_1'=4] {'tp_0','tp_1'}, dimensions={0} | all-to-all | bytes 1310720 | tf_op jit(solution)/shard_map/all_to_all | solution.py:356
  98.5 0.3 shard_map.150
  98.8 21.3 %all_to_all.35 = bf16[32,8,128]{2,1,0:T(8,128)(2,1)S(1)} all-to-all(bf16[32,8,128]{2,1,0:T(8,128)(2,1)S(1)} %bitcast.16), channel_id=1, replica_groups=mesh['sp'=32,'tp_0'=4,'tp_1'=4] {'sp'}, dimensions={0} | all-to-all | bytes 131072 | tf_op jit(solution)/shard_map/all_to_all | solution.py:356
  120.1 0.9 shard_map.151
Async XLA Ops:
  34.4 16.4 %copy-start.3 = (bf16[64,128]{1,0:T(8,128)(2,1)S(1)}, bf16[64,128]{1,0:T(8,128)(2,1)}, u32[]{:S(2)}) copy-start(bf16[64,128]{1,0:T(8,128)(2,1)} %residual_ref.1) | copy-start | bytes 49156
  34.4 16.4 %copy-start.4 = (s32[64,2]{0,1:T(2,128)S(1)}, s32[64,2]{0,1:T(2,128)}, u32[]{:S(2)}) copy-start(s32[64,2]{0,1:T(2,128)} %param.25) | copy-start | bytes 1540
  34.4 16.4 %copy-start.5 = (f32[64,2]{0,1:T(2,128)S(1)}, f32[64,2]{0,1:T(2,128)}, u32[]{:S(2)}) copy-start(f32[64,2]{0,1:T(2,128)} %param.26) | copy-start | bytes 1540
  34.4 35.2 %copy-start.6 = (f32[128]{0:T(128)S(1)}, f32[128]{0:T(128)}, u32[]{:S(2)}) copy-start(f32[128]{0:T(128)} %param.24) | copy-start | bytes 1540
  36.5 48.0 %copy-start.2 = (bf16[1,256,2048]{2,1,0:T(8,128)(2,1)S(1)}, bf16[1,256,2048]{2,1,0:T(8,128)(2,1)}, u32[]{:S(2)}) copy-start(bf16[1,256,2048]{2,1,0:T(8,128)(2,1)} %down_ref.1) | copy-start | bytes 3145732
  69.6 14.8 %copy-start = (bf16[1,2048,256]{2,1,0:T(8,128)(2,1)S(1)}, bf16[1,2048,256]{2,1,0:T(8,128)(2,1)}, u32[]{:S(2)}) copy-start(bf16[1,2048,256]{2,1,0:T(8,128)(2,1)} %gate_ref.1) | copy-start | bytes 3145732
  69.7 14.8 %copy-start.1 = (bf16[1,2048,256]{2,1,0:T(8,128)(2,1)S(1)}, bf16[1,2048,256]{2,1,0:T(8,128)(2,1)}, u32[]{:S(2)}) copy-start(bf16[1,2048,256]{2,1,0:T(8,128)(2,1)} %up_ref.1) | copy-start | bytes 3145732

commit v4 on v3

--- a/solution.py
+++ b/solution.py
@@ -18,7 +18,8 @@
 ROWS = 64
 GROUPS = 8
 SLOTS = 5
-PAD = 8
+PAD = 6
+LINES = 10
 EROWS = BLOCKS * SLOTS
 SENT = EROWS + 16
 
@@ -54,6 +55,10 @@
 
 def iota(shape, dim):
     return lax.broadcasted_iota(jnp.int32, shape, dim)
+
+
+def divided(x, by):
+    return (x * (65536 // by + 1)) >> 16
 
 
 def mm(a, b):
@@ -157,34 +162,37 @@
             (by_sin * real + new_imag) + by_cos * imag,
         )
         total = total * keep
-    crossed = pltpu.roll(total, 64, 1)
-    high = crossed.astype(bf16).astype(f32)
-    decay = jnp.where((lane & 32) == 0, high, crossed - high)
+    high = total.astype(bf16).astype(f32)
+    low = total - high
     first_doc = docs_ref[0].astype(f32)
     last_doc = docs_ref[ROWS - 1].astype(f32)
     turn_ref[2] = jnp.where(fwd, first_doc, last_doc)
-    to_later = jnp.concatenate(
-        [jnp.where(fwd, real, decay), jnp.where(fwd, imag, last_doc)], axis=0
-    ).astype(bf16)
-    to_earlier = jnp.concatenate(
-        [jnp.where(fwd, decay, real), jnp.where(fwd, first_doc, imag)], axis=0
-    ).astype(bf16)
-    me = me_ref[0]
-    for i in range(BLOCKS):
-        @pl.when(me < i)
-        def _():
-            message_ref[i] = to_later
-
-        @pl.when(me >= i)
-        def _():
-            message_ref[i] = to_earlier
+    group = iota((GROUPS, 128), 0)
+    lines = []
+    for kept, doc, left, right in [
+        (0, last_doc, real, pltpu.roll(imag, 64, 1)),
+        (64, first_doc, pltpu.roll(imag, 64, 1), real),
+    ]:
+        decays = jnp.where(lane == kept + group, high, 0.0) + jnp.where(
+            lane == kept + GROUPS + group, low, 0.0
+        )
+        row = jnp.sum(decays, axis=0, keepdims=True) + jnp.where(
+            lane[0:1] == kept + 2 * GROUPS, doc, 0.0
+        )
+        lines.append(jnp.where(fwd, left, right))
+        lines.append(jnp.broadcast_to(row, (GROUPS, 128)))
+    lines = jnp.concatenate(lines, axis=0).astype(bf16)
+    row, entry = iota((BLOCKS * LINES, 32), 0), iota((BLOCKS * LINES, 32), 1)
+    receiver = divided(row, LINES)
+    wanted = row - receiver * LINES + jnp.where(receiver > me_ref[0], 0, 16)
+    message_ref[...] = mm((entry == wanted).astype(f32).astype(bf16), lines).astype(bf16)
 
 
 def mixer_body(
-    me_ref, message_ref, real_ref, imag_ref, keep_ref, turn_ref,
+    me_ref, messages_ref, real_ref, imag_ref, keep_ref, turn_ref,
     far_x, far_read, far_skip, far_weight,
     partial_ref,
-    states, read_out, x_ref, read_mix_ref, skip_ref, out_weight_ref, arrivals,
+    states, read_out, received, x_ref, read_mix_ref, skip_ref, out_weight_ref, arrivals,
 ):
     here_now = [
         pltpu.make_async_copy(far, near_ref, arrivals.at[k])
@@ -196,7 +204,6 @@
         copy.start()
     lane = iota((GROUPS, 128), 1)
     fwd = lane < 64
-    odd = (lane & 32) != 0
     me = me_ref[0]
     cos, sin, mine = turn_ref[0], turn_ref[1], turn_ref[2]
     block_cos, block_sin = cos, sin
@@ -205,17 +212,27 @@
             block_cos * block_cos - block_sin * block_sin,
             2.0 * block_cos * block_sin,
         )
+    row, entry = iota((BLOCKS * 16, BLOCKS * LINES), 0), iota((BLOCKS * 16, BLOCKS * LINES), 1)
+    wanted = (row >> 4) * LINES + jnp.minimum(row & 15, LINES - 1)
+    received[...] = mm((entry == wanted).astype(f32).astype(bf16), messages_ref[...])
+    group = iota((GROUPS, 128), 0)
+    decays, docs = [], []
+    for n in range(BLOCKS):
+        kept = received[16 * n + GROUPS : 16 * (n + 1), :]
+        place = lane & 63
+        of_group = (place == group) | (place == GROUPS + group)
+        decays.append(jnp.sum(jnp.where(of_group, kept, 0.0), axis=1, keepdims=True))
+        docs.append(jnp.sum(jnp.where(place == 2 * GROUPS, kept, 0.0), axis=1, keepdims=True))
     real = jnp.zeros((GROUPS, 128), f32)
     imag = jnp.zeros((GROUPS, 128), f32)
     for n in range(BLOCKS - 1):
         r = BLOCKS - 1 - n
-        one, two = message_ref[n].astype(f32), message_ref[r].astype(f32)
-        decay = pltpu.roll(jnp.where(fwd, two[:GROUPS], one[:GROUPS]), 64, 1)
-        decay = decay + jnp.where(odd, pltpu.roll(decay, 32, 1), pltpu.roll(decay, 96, 1))
-        doc = pltpu.roll(jnp.where(fwd, two[GROUPS:], one[GROUPS:]), 64, 1)
-        same = doc == mine
-        new_real = jnp.where(same, jnp.where(fwd, one[:GROUPS], two[:GROUPS]), 0.0)
-        new_imag = jnp.where(same, jnp.where(fwd, one[GROUPS:], two[GROUPS:]), 0.0)
+        one = received[16 * n : 16 * n + GROUPS, :]
+        two = received[16 * r : 16 * r + GROUPS, :]
+        decay = jnp.where(fwd, decays[n], decays[r])
+        same = jnp.where(fwd, docs[n], docs[r]) == mine
+        new_real = jnp.where(same, jnp.where(fwd, one, two), 0.0)
+        new_imag = jnp.where(same, pltpu.roll(jnp.where(fwd, two, one), 64, 1), 0.0)
         by_cos, by_sin = decay * block_cos, decay * block_sin
         passed = jnp.where(fwd, (n < me).astype(jnp.int32), (r > me).astype(jnp.int32)) > 0
         real, imag = (
@@ -294,7 +311,7 @@
 
 def packed_rows(shape, packed_dim):
     packed, padded = iota(shape, packed_dim), iota(shape, 1 - packed_dim)
-    block = padded // PAD
+    block = divided(padded, PAD)
     slot = padded - block * PAD
     return ((slot < SLOTS) & (packed == block * SLOTS + slot)).astype(f32).astype(bf16)
 
@@ -354,6 +371,11 @@
 
 def exchanged(pieces, axis):
     return lax.all_to_all(pieces, axis, 0, 0, tiled=True)
+
+
+def rows_exchanged(rows):
+    pairs = rows.reshape(BLOCKS, rows.shape[0] // (2 * BLOCKS), 2, rows.shape[1])
+    return exchanged(pairs, "sp").reshape(rows.shape)
 
 
 def shards(
@@ -379,7 +401,7 @@
         sweep_body,
         [SMEM, FAR, FAR, FAR, FAR, FAR],
         [
-            ((BLOCKS, 16, 128), bf16),
+            ((BLOCKS * LINES, 128), bf16),
             ((ROWS, GROUPS, 128), f32),
             ((ROWS, GROUPS, 128), f32),
             ((ROWS, GROUPS, 128), f32),
@@ -399,7 +421,7 @@
     )(
         me, far(doc_ids), far(log_step), far(log_extra.T), far(mixer_in), far(in_mix.reshape(2, 128, 128))
     )
-    messages = near(exchanged(message, "sp"))
+    messages = near(rows_exchanged(message))
     (partial,) = call(
         mixer_body,
         [SMEM] + [VMEM] * 5 + [FAR] * 4,
@@ -407,6 +429,7 @@
         [
             ((2, tall, 128), f32),
             ((tall, 128), f32),
+            ((BLOCKS * 16, 128), f32),
             ((ROWS, 128), bf16),
             ((2, 128, 128), f32),
             ((1, 128), f32),
@@ -424,7 +447,7 @@
         [VMEM] * 4,
         [((ROWS, 128), bf16), ((BLOCKS * PAD, 128), bf16), ((2, ROWS), f32)],
     )(shares, residual, routes.T, route_weight.T)
-    arrived = exchanged(outgoing.reshape(BLOCKS, PAD, 128), "sp").reshape(BLOCKS * PAD, 128)
+    arrived = rows_exchanged(outgoing)
     (copies,) = call(copies_body, [VMEM] * 2, [((PEERS, SENT, 128), bf16)])(
         near(arrived), norm_gain.reshape(1, 128)
     )
@@ -437,7 +460,7 @@
     (answer,) = call(answer_body, [VMEM], [((BLOCKS * PAD, 128), bf16)])(
         near(exchanged(terms, TP))
     )
-    returned = exchanged(answer.reshape(BLOCKS, PAD, 128), "sp").reshape(BLOCKS * PAD, 128)
+    returned = rows_exchanged(answer)
     (out,) = call(mixture_body, [VMEM] * 4, [((ROWS, 128), bf16)], last=True)(
         near(returned), near(stream), routes.T, near(weights)
     )

time: 121 us -> 119 us (0.983)
  blocking collectives: 114 us -> 111 us
  local copies, waits for them, and re-layouts: 0.03 us -> 1.35 us
    all_to_all x6, blocking collectives: 114 us -> 111 us  [exchanged(): return lax.all_to_all(pieces, axis, 0, 0, tiled=True)]
    unnamed x14, local copies, waits for them, and re-layouts: 0.03 us -> 1.35 us
where the time goes in v4:
time: 119 us
  blocking collectives  111 us (93%)
  Pallas kernels  6.62 us (6%)
  local copies, waits for them, and re-layouts  1.35 us (1%)
    all_to_all x6, blocking collectives, exchanged(): return lax.all_to_all(pieces, axis, 0, 0, tiled=True)  111 us
    pallas_call x1, Pallas kernels, shards(): call(mixer_body, [SMEM] + [VMEM] * 5 + [FAR] * 4, [((PEERS, ROWS, 128), b...  2.39 us

profile of v4, /device:TPU:1, one launch (start us, length us, event | category | flops | bytes accessed | tf_op | source)
XLA Modules:
  0.0 118.7 jit_solution(16070350425180430034)
XLA Ops:
  0.0 1.7 %shard_map.145 = (bf16[320,128]{1,0:T(8,128)(2,1)S(1)}, f32[64,8,128]{2,1,0:T(8,128)S(1)}, f32[64,8,128]{2,1,0:T(8,128)S(1)}, f32[64,8,128]{2,1,0:T(8,128)S(1)}, f32[3,8,128]{2,1,0:T(8,128)S(1)}) custom-call(s32[1]{0:T(128)} %bitcast.me_ref, s32[64]{0:T(128)} %far_docs.1, f32[2,8]{1,0:T(2,128)} %far_step.1, f32[8,64]{1,0:T(8,128)} %bitcast.28, ...), custom_call_target="tpu_custom_call" | custom-call | tf_op jit(solution)/shard_map/pallas_call | solution.py:400
  1.7 30.3 %all_to_all.30 = bf16[32,5,2,128]{3,2,1,0:T(2,128)(2,1)S(1)} all-to-all(bf16[32,5,2,128]{3,2,1,0:T(2,128)(2,1)S(1)} %bitcast.20), channel_id=1, replica_groups=mesh['sp'=32,'tp_0'=4,'tp_1'=4] {'sp'}, dimensions={0} | all-to-all | bytes 163840 | tf_op jit(solution)/shard_map/all_to_all | solution.py:373
  32.0 0.0 copy-start.2
  32.0 2.4 %shard_map.146 = bf16[16,64,128]{2,1,0:T(8,128)(2,1)S(1)} custom-call(s32[1]{0:T(128)} %bitcast.me_ref, bf16[320,128]{1,0:T(8,128)(2,1)S(1)} %bitcast.16, f32[64,8,128]{2,1,0:T(8,128)S(1)} %get-tuple-element.14.real_ref, f32[64,8,128]{2,1,0:T(8,128)S(1)} %get-tuple-element.15.imag_ref, f32[64,8,128]{2,1,0:T(8,128)S(1)} %get-tuple-element.16.keep_ref, ...), custom_call_target="tpu_custom_call" | custom-call | tf_op jit(solution)/shard_map/pallas_call | solution.py:425
  34.4 0.0 copy-start.3
  34.4 0.0 copy-start.5
  34.4 14.1 %all_to_all.31.arrived_ref = bf16[16,64,128]{2,1,0:T(8,128)(2,1)S(1)} all-to-all(bf16[16,64,128]{2,1,0:T(8,128)(2,1)S(1)} %shard_map.146), channel_id=1, replica_groups=mesh['sp'=32,'tp_0'=4,'tp_1'=4] {'tp_0','tp_1'}, dimensions={0} | all-to-all | bytes 524288 | tf_op jit(solution)/shard_map/all_to_all | solution.py:373
  48.5 0.0 copy-start.4
  48.5 0.0 copy-done.3
  48.5 0.0 copy-done.5
  48.5 0.7 copy-done.4
  49.2 0.2 shard_map.147
  49.4 18.2 %all_to_all.32 = bf16[32,3,2,128]{3,2,1,0:T(2,128)(2,1)S(1)} all-to-all(bf16[32,3,2,128]{3,2,1,0:T(2,128)(2,1)S(1)} %bitcast.21), channel_id=1, replica_groups=mesh['sp'=32,'tp_0'=4,'tp_1'=4] {'sp'}, dimensions={0} | all-to-all | bytes 98304 | tf_op jit(solution)/shard_map/all_to_all | solution.py:373
  67.6 0.0 copy-start.6
  67.6 0.7 copy-done.6
  68.3 0.0 copy-start
  68.3 0.0 copy-start.1
  68.3 0.2 shard_map.148
  68.5 14.6 %all_to_all.33.rows_ref = bf16[16,176,128]{2,1,0:T(8,128)(2,1)S(1)} all-to-all(bf16[16,176,128]{2,1,0:T(8,128)(2,1)S(1)} %shard_map.148), channel_id=1, replica_groups=mesh['sp'=32,'tp_0'=4,'tp_1'=4] {'tp_0','tp_1'}, dimensions={0} | all-to-all | bytes 1441792 | tf_op jit(solution)/shard_map/all_to_all | solution.py:373
  83.0 0.0 copy-done.2
  83.0 0.0 copy-done
  83.0 0.0 copy-done.1
  83.0 0.9 shard_map.149
  84.0 13.1 %all_to_all.34.terms_ref = bf16[16,160,128]{2,1,0:T(8,128)(2,1)S(1)} all-to-all(bf16[16,160,128]{2,1,0:T(8,128)(2,1)S(1)} %shard_map.149), channel_id=1, replica_groups=mesh['sp'=32,'tp_0'=4,'tp_1'=4] {'tp_0','tp_1'}, dimensions={0} | all-to-all | bytes 1310720 | tf_op jit(solution)/shard_map/all_to_all | solution.py:373
  97.1 0.2 shard_map.150
  97.4 20.4 %all_to_all.35 = bf16[32,3,2,128]{3,2,1,0:T(2,128)(2,1)S(1)} all-to-all(bf16[32,3,2,128]{3,2,1,0:T(2,128)(2,1)S(1)} %bitcast.19), channel_id=1, replica_groups=mesh['sp'=32,'tp_0'=4,'tp_1'=4] {'sp'}, dimensions={0} | all-to-all | bytes 98304 | tf_op jit(solution)/shard_map/all_to_all | solution.py:373
  117.8 0.9 shard_map.151
Async XLA Ops:
  32.0 51.1 %copy-start.2 = (bf16[1,256,2048]{2,1,0:T(8,128)(2,1)S(1)}, bf16[1,256,2048]{2,1,0:T(8,128)(2,1)}, u32[]{:S(2)}) copy-start(bf16[1,256,2048]{2,1,0:T(8,128)(2,1)} %down_ref.1) | copy-start | bytes 3145732
  34.4 14.2 %copy-start.3 = (bf16[64,128]{1,0:T(8,128)(2,1)S(1)}, bf16[64,128]{1,0:T(8,128)(2,1)}, u32[]{:S(2)}) copy-start(bf16[64,128]{1,0:T(8,128)(2,1)} %residual_ref.1) | copy-start | bytes 49156
  34.4 14.2 %copy-start.5 = (f32[64,2]{0,1:T(2,128)S(1)}, f32[64,2]{0,1:T(2,128)}, u32[]{:S(2)}) copy-start(f32[64,2]{0,1:T(2,128)} %param.26) | copy-start | bytes 1540
  48.5 0.7 copy-start.4
  67.6 0.7 copy-start.6
  68.3 14.8 %copy-start = (bf16[1,2048,256]{2,1,0:T(8,128)(2,1)S(1)}, bf16[1,2048,256]{2,1,0:T(8,128)(2,1)}, u32[]{:S(2)}) copy-start(bf16[1,2048,256]{2,1,0:T(8,128)(2,1)} %gate_ref.1) | copy-start | bytes 3145732
  68.3 14.8 %copy-start.1 = (bf16[1,2048,256]{2,1,0:T(8,128)(2,1)S(1)}, bf16[1,2048,256]{2,1,0:T(8,128)(2,1)}, u32[]{:S(2)}) copy-start(bf16[1,2048,256]{2,1,0:T(8,128)(2,1)} %up_ref.1) | copy-start | bytes 3145732

commit v5 on v4

--- a/solution.py
+++ b/solution.py
@@ -20,6 +20,7 @@
 SLOTS = 5
 PAD = 6
 LINES = 10
+LATER = 8
 EROWS = BLOCKS * SLOTS
 SENT = EROWS + 16
 
@@ -99,26 +100,29 @@
 
 
 def sweep_body(
-    me_ref, far_docs, far_step, far_extra, far_x, far_mix,
-    message_ref, real_ref, imag_ref, keep_ref, turn_ref,
-    masked, source, magnitude, log_step_ref, log_extra_ref, x_ref, in_mix_ref, docs_ref, arrivals,
+    me_ref, far_docs, far_step, far_extra, far_mix, *refs
 ):
-    here_now = [
-        pltpu.make_async_copy(far, near_ref, arrivals.at[k])
-        for k, (far, near_ref) in enumerate(
-            [
-                (far_mix, in_mix_ref),
-                (far_x, x_ref),
-                (far_extra, log_extra_ref),
-                (far_step, log_step_ref),
-                (far_docs, docs_ref),
-            ]
-        )
+    far_later, refs = refs[:LATER], refs[LATER:]
+    message_ref, real_ref, imag_ref, keep_ref, turn_ref = refs[:5]
+    later, refs = refs[5 : 5 + LATER], refs[5 + LATER :]
+    masked, source, magnitude, log_step_ref, log_extra_ref, in_mix_ref, docs_ref, arrivals = refs
+    x_ref = later[0]
+    pairs = [
+        (far_mix, in_mix_ref),
+        (far_later[0], x_ref),
+        (far_extra, log_extra_ref),
+        (far_step, log_step_ref),
+        (far_docs, docs_ref),
+        *zip(far_later[1:], later[1:]),
     ]
-    for copy in here_now:
-        copy.start()
-    for copy in here_now[::-1]:
-        copy.wait()
+    fetches = [
+        pltpu.make_async_copy(distant, local, arrivals.at[k])
+        for k, (distant, local) in enumerate(pairs)
+    ]
+    for fetch in fetches:
+        fetch.start()
+    for fetch in fetches[:5]:
+        fetch.wait()
     lane = iota((GROUPS, 128), 1)
     fwd = lane < 64
     step = steps_by_lane(log_step_ref[...])
@@ -186,22 +190,16 @@
     receiver = divided(row, LINES)
     wanted = row - receiver * LINES + jnp.where(receiver > me_ref[0], 0, 16)
     message_ref[...] = mm((entry == wanted).astype(f32).astype(bf16), lines).astype(bf16)
+    for fetch in fetches[5:]:
+        fetch.wait()
 
 
 def mixer_body(
     me_ref, messages_ref, real_ref, imag_ref, keep_ref, turn_ref,
-    far_x, far_read, far_skip, far_weight,
+    x_ref, read_mix_ref, skip_ref, out_weight_ref,
     partial_ref,
-    states, read_out, received, x_ref, read_mix_ref, skip_ref, out_weight_ref, arrivals,
+    states, read_out, received, spread,
 ):
-    here_now = [
-        pltpu.make_async_copy(far, near_ref, arrivals.at[k])
-        for k, (far, near_ref) in enumerate(
-            [(far_read, read_mix_ref), (far_x, x_ref), (far_skip, skip_ref), (far_weight, out_weight_ref)]
-        )
-    ]
-    for copy in here_now:
-        copy.start()
     lane = iota((GROUPS, 128), 1)
     fwd = lane < 64
     me = me_ref[0]
@@ -212,25 +210,29 @@
             block_cos * block_cos - block_sin * block_sin,
             2.0 * block_cos * block_sin,
         )
-    row, entry = iota((BLOCKS * 16, BLOCKS * LINES), 0), iota((BLOCKS * 16, BLOCKS * LINES), 1)
-    wanted = (row >> 4) * LINES + jnp.minimum(row & 15, LINES - 1)
-    received[...] = mm((entry == wanted).astype(f32).astype(bf16), messages_ref[...])
-    group = iota((GROUPS, 128), 0)
-    decays, docs = [], []
-    for n in range(BLOCKS):
-        kept = received[16 * n + GROUPS : 16 * (n + 1), :]
-        place = lane & 63
-        of_group = (place == group) | (place == GROUPS + group)
-        decays.append(jnp.sum(jnp.where(of_group, kept, 0.0), axis=1, keepdims=True))
-        docs.append(jnp.sum(jnp.where(place == 2 * GROUPS, kept, 0.0), axis=1, keepdims=True))
+    received[...] = messages_ref[...].astype(f32)
+    place, group = lane & 63, iota((GROUPS, 128), 0)
+    of_group = (place == group) | (place == GROUPS + group) | (place == 2 * GROUPS)
+    scalars = jnp.concatenate(
+        [
+            jnp.where(of_group, received[LINES * n + GROUPS : LINES * n + GROUPS + 1, :], 0.0)
+            for n in range(BLOCKS)
+        ],
+        axis=0,
+    ).astype(bf16)
+    entry = iota((128, 256), 0) & 63
+    left = iota((128, 256), 1) < 128
+    summed = (left & (entry < 2 * GROUPS)) | (~left & (entry == 2 * GROUPS))
+    spread[...] = mm(scalars, summed.astype(f32).astype(bf16))
     real = jnp.zeros((GROUPS, 128), f32)
     imag = jnp.zeros((GROUPS, 128), f32)
     for n in range(BLOCKS - 1):
         r = BLOCKS - 1 - n
-        one = received[16 * n : 16 * n + GROUPS, :]
-        two = received[16 * r : 16 * r + GROUPS, :]
-        decay = jnp.where(fwd, decays[n], decays[r])
-        same = jnp.where(fwd, docs[n], docs[r]) == mine
+        one = received[LINES * n : LINES * n + GROUPS, :]
+        two = received[LINES * r : LINES * r + GROUPS, :]
+        here, there = pl.ds(GROUPS * n, GROUPS), pl.ds(GROUPS * r, GROUPS)
+        decay = jnp.where(fwd, spread[here, 0:128], spread[there, 0:128])
+        same = jnp.where(fwd, spread[here, 128:256], spread[there, 128:256]) == mine
         new_real = jnp.where(same, jnp.where(fwd, one, two), 0.0)
         new_imag = jnp.where(same, pltpu.roll(jnp.where(fwd, two, one), 64, 1), 0.0)
         by_cos, by_sin = decay * block_cos, decay * block_sin
@@ -252,8 +254,6 @@
         states[0, there, 64:128] = real[:, 64:128]
         states[1, here, 0:64] = imag[:, 0:64]
         states[1, there, 64:128] = imag[:, 64:128]
-    for copy in here_now:
-        copy.wait()
     read_real, read_imag = halves_joined(read_mix_ref[0], read_mix_ref[1])
     read_out[...] = mm_across(states[0].astype(bf16), read_real.astype(bf16)) + mm_across(
         states[1].astype(bf16), read_imag.astype(bf16)
@@ -291,10 +291,7 @@
     return expert * PAD + rank
 
 
-def stream_body(
-    arrived_ref, residual_ref, routes_ref, weight_ref, stream_ref, outgoing_ref, weights_ref
-):
-    weights_ref[...] = weight_ref[...]
+def stream_body(arrived_ref, residual_ref, routes_ref, stream_ref, outgoing_ref):
     total = residual_ref[...].astype(f32)
     projected = arrived_ref[0].astype(f32)
     for j in range(1, PEERS):
@@ -397,15 +394,26 @@
 ):
     me = lax.axis_index("sp").reshape(1)
     tall = GROUPS * ROWS
-    message, real, imag, keep, turn = call(
+    later = (
+        mixer_in,
+        read_mix.swapaxes(2, 3).reshape(2, 128, 128),
+        skip_gain.reshape(1, 128),
+        out_weight,
+        residual,
+        routes.T,
+        route_weight.T,
+        norm_gain.reshape(1, 128),
+    )
+    message, real, imag, keep, turn, *later = call(
         sweep_body,
-        [SMEM, FAR, FAR, FAR, FAR, FAR],
+        [SMEM] + [FAR] * (4 + LATER),
         [
             ((BLOCKS * LINES, 128), bf16),
             ((ROWS, GROUPS, 128), f32),
             ((ROWS, GROUPS, 128), f32),
             ((ROWS, GROUPS, 128), f32),
             ((3, GROUPS, 128), f32),
+            *((x.shape, x.dtype) for x in later),
         ],
         [
             ((tall, 128), f32),
@@ -413,43 +421,41 @@
             ((tall, 128), f32),
             ((2, GROUPS), f32),
             ((GROUPS, ROWS), f32),
-            ((ROWS, 128), bf16),
             ((2, 128, 128), f32),
             ((ROWS,), jnp.int32),
         ],
-        copies=5,
+        copies=4 + LATER,
     )(
-        me, far(doc_ids), far(log_step), far(log_extra.T), far(mixer_in), far(in_mix.reshape(2, 128, 128))
+        me, far(doc_ids), far(log_step), far(log_extra.T), far(in_mix.reshape(2, 128, 128)),
+        *map(far, later),
+    )
+    mixer_in, read_mix, skip_gain, out_weight, residual, routes, route_weight, norm_gain = map(
+        near, later
     )
     messages = near(rows_exchanged(message))
     (partial,) = call(
         mixer_body,
-        [SMEM] + [VMEM] * 5 + [FAR] * 4,
+        [SMEM] + [VMEM] * 9,
         [((PEERS, ROWS, 128), bf16)],
         [
             ((2, tall, 128), f32),
             ((tall, 128), f32),
-            ((BLOCKS * 16, 128), f32),
-            ((ROWS, 128), bf16),
-            ((2, 128, 128), f32),
-            ((1, 128), f32),
-            ((128, 128 * PEERS), bf16),
+            ((BLOCKS * LINES, 128), f32),
+            ((BLOCKS * GROUPS, 256), f32),
         ],
-        copies=4,
     )(
-        me, messages, near(real), near(imag), near(keep), near(turn), far(mixer_in),
-        far(read_mix.swapaxes(2, 3).reshape(2, 128, 128)), far(skip_gain.reshape(1, 128)),
-        far(out_weight),
+        me, messages, near(real), near(imag), near(keep), near(turn),
+        mixer_in, read_mix, skip_gain, out_weight,
     )
     shares = near(exchanged(partial, TP))
-    stream, outgoing, weights = call(
+    stream, outgoing = call(
         stream_body,
-        [VMEM] * 4,
-        [((ROWS, 128), bf16), ((BLOCKS * PAD, 128), bf16), ((2, ROWS), f32)],
-    )(shares, residual, routes.T, route_weight.T)
+        [VMEM] * 3,
+        [((ROWS, 128), bf16), ((BLOCKS * PAD, 128), bf16)],
+    )(shares, residual, routes)
     arrived = rows_exchanged(outgoing)
     (copies,) = call(copies_body, [VMEM] * 2, [((PEERS, SENT, 128), bf16)])(
-        near(arrived), norm_gain.reshape(1, 128)
+        near(arrived), norm_gain
     )
     (terms,) = call(
         expert_body,
@@ -462,7 +468,7 @@
     )
     returned = rows_exchanged(answer)
     (out,) = call(mixture_body, [VMEM] * 4, [((ROWS, 128), bf16)], last=True)(
-        near(returned), near(stream), routes.T, near(weights)
+        near(returned), near(stream), routes, route_weight
     )
     return out
 

time: 119 us -> 116 us (0.975)
  local copies, waits for them, and re-layouts: 1.35 us -> 0.01 us
  Pallas kernels: 6.62 us -> 5.36 us
    unnamed x14 -> x6, local copies, waits for them, and re-layouts: 1.35 us -> 0.01 us
    pallas_call x3, Pallas kernels: 4.33 us -> 3.07 us  [the longest x1 1.79 us: shards(): call(sweep_body, [SMEM] + [FAR] * (4 + LATER), [((BLOCKS * LINES, 128), b...]
where the time goes in v5:
time: 116 us
  blocking collectives  111 us (96%)
  Pallas kernels  5.36 us (5%)
    all_to_all x6, blocking collectives, exchanged(): return lax.all_to_all(pieces, axis, 0, 0, tiled=True)  111 us

profile of v5, /device:TPU:1, one launch (start us, length us, event | category | flops | bytes accessed | tf_op | source)
XLA Modules:
  0.0 116.1 jit_solution(10920975627081980304)
XLA Ops:
  0.0 1.8 %shard_map.145 = (bf16[320,128]{1,0:T(8,128)(2,1)S(1)}, f32[64,8,128]{2,1,0:T(8,128)S(1)}, f32[64,8,128]{2,1,0:T(8,128)S(1)}, f32[64,8,128]{2,1,0:T(8,128)S(1)},...) custom-call(s32[1]{0:T(128)} %bitcast.me_ref, ...), custom_call_target="tpu_custom_call" | custom-call | tf_op jit(solution)/shard_map/pallas_call | solution.py:407
  1.8 30.3 %all_to_all.30 = bf16[32,5,2,128]{3,2,1,0:T(2,128)(2,1)S(1)} all-to-all(bf16[32,5,2,128]{3,2,1,0:T(2,128)(2,1)S(1)} %bitcast.20), channel_id=1, replica_groups=mesh['sp'=32,'tp_0'=4,'tp_1'=4] {'sp'}, dimensions={0} | all-to-all | bytes 163840 | tf_op jit(solution)/shard_map/all_to_all | solution.py:370
  32.0 0.0 copy-start.2
  32.0 1.0 shard_map.146
  33.1 14.1 %all_to_all.31.arrived_ref = bf16[16,64,128]{2,1,0:T(8,128)(2,1)S(1)} all-to-all(bf16[16,64,128]{2,1,0:T(8,128)(2,1)S(1)} %shard_map.146), channel_id=1, replica_groups=mesh['sp'=32,'tp_0'=4,'tp_1'=4] {'tp_0','tp_1'}, dimensions={0} | all-to-all | bytes 524288 | tf_op jit(solution)/shard_map/all_to_all | solution.py:370
  47.2 0.2 shard_map.147
  47.5 18.2 %all_to_all.32 = bf16[32,3,2,128]{3,2,1,0:T(2,128)(2,1)S(1)} all-to-all(bf16[32,3,2,128]{3,2,1,0:T(2,128)(2,1)S(1)} %bitcast.21), channel_id=1, replica_groups=mesh['sp'=32,'tp_0'=4,'tp_1'=4] {'sp'}, dimensions={0} | all-to-all | bytes 98304 | tf_op jit(solution)/shard_map/all_to_all | solution.py:370
  65.6 0.0 copy-start
  65.6 0.0 copy-start.1
  65.6 0.2 shard_map.148
  65.8 14.6 %all_to_all.33.rows_ref = bf16[16,176,128]{2,1,0:T(8,128)(2,1)S(1)} all-to-all(bf16[16,176,128]{2,1,0:T(8,128)(2,1)S(1)} %shard_map.148), channel_id=1, replica_groups=mesh['sp'=32,'tp_0'=4,'tp_1'=4] {'tp_0','tp_1'}, dimensions={0} | all-to-all | bytes 1441792 | tf_op jit(solution)/shard_map/all_to_all | solution.py:370
  80.4 0.0 copy-done.2
  80.4 0.0 copy-done
  80.4 0.0 copy-done.1
  80.4 0.9 shard_map.149
  81.4 13.1 %all_to_all.34.terms_ref = bf16[16,160,128]{2,1,0:T(8,128)(2,1)S(1)} all-to-all(bf16[16,160,128]{2,1,0:T(8,128)(2,1)S(1)} %shard_map.149), channel_id=1, replica_groups=mesh['sp'=32,'tp_0'=4,'tp_1'=4] {'tp_0','tp_1'}, dimensions={0} | all-to-all | bytes 1310720 | tf_op jit(solution)/shard_map/all_to_all | solution.py:370
  94.5 0.2 shard_map.150
  94.8 20.4 %all_to_all.35 = bf16[32,3,2,128]{3,2,1,0:T(2,128)(2,1)S(1)} all-to-all(bf16[32,3,2,128]{3,2,1,0:T(2,128)(2,1)S(1)} %bitcast.19), channel_id=1, replica_groups=mesh['sp'=32,'tp_0'=4,'tp_1'=4] {'sp'}, dimensions={0} | all-to-all | bytes 98304 | tf_op jit(solution)/shard_map/all_to_all | solution.py:370
  115.2 0.9 shard_map.151
Async XLA Ops:
  32.0 48.4 %copy-start.2 = (bf16[1,256,2048]{2,1,0:T(8,128)(2,1)S(1)}, bf16[1,256,2048]{2,1,0:T(8,128)(2,1)}, u32[]{:S(2)}) copy-start(bf16[1,256,2048]{2,1,0:T(8,128)(2,1)} %down_ref.1) | copy-start | bytes 3145732
  65.6 14.8 %copy-start = (bf16[1,2048,256]{2,1,0:T(8,128)(2,1)S(1)}, bf16[1,2048,256]{2,1,0:T(8,128)(2,1)}, u32[]{:S(2)}) copy-start(bf16[1,2048,256]{2,1,0:T(8,128)(2,1)} %gate_ref.1) | copy-start | bytes 3145732
  65.6 14.8 %copy-start.1 = (bf16[1,2048,256]{2,1,0:T(8,128)(2,1)S(1)}, bf16[1,2048,256]{2,1,0:T(8,128)(2,1)}, u32[]{:S(2)}) copy-start(bf16[1,2048,256]{2,1,0:T(8,128)(2,1)} %up_ref.1) | copy-start | bytes 3145732

commit v6 on v5

--- a/solution.py
+++ b/solution.py
@@ -20,9 +20,11 @@
 SLOTS = 5
 PAD = 6
 LINES = 10
+SPANS = 4
+SQUARED = 4
 LATER = 8
 EROWS = BLOCKS * SLOTS
-SENT = EROWS + 16
+SENT = EROWS + 4
 
 VMEM = pl.BlockSpec(memory_space=pltpu.VMEM)
 SMEM = pl.BlockSpec(memory_space=pltpu.SMEM)
@@ -92,6 +94,19 @@
     return jnp.where(iota((GROUPS, 128), 1) < 64, columns[0], columns[1])
 
 
+def turned(by_cos, by_sin, real, imag, new_real, new_imag):
+    return (
+        (by_cos * real + new_real) - by_sin * imag,
+        (by_sin * real + new_imag) + by_cos * imag,
+    )
+
+
+def raised(cos, sin, squarings):
+    for _ in range(squarings):
+        cos, sin = cos * cos - sin * sin, 2.0 * cos * sin
+    return cos, sin
+
+
 def one_minus_exp(x):
     series = jnp.ones_like(x)
     for n in range(9, 1, -1):
@@ -103,16 +118,16 @@
     me_ref, far_docs, far_step, far_extra, far_mix, *refs
 ):
     far_later, refs = refs[:LATER], refs[LATER:]
-    message_ref, real_ref, imag_ref, keep_ref, turn_ref = refs[:5]
-    later, refs = refs[5 : 5 + LATER], refs[5 + LATER :]
+    message_ref, real_ref, imag_ref, keep_ref, turn_ref, span_ref = refs[:6]
+    later, refs = refs[6 : 6 + LATER], refs[6 + LATER :]
     masked, source, magnitude, log_step_ref, log_extra_ref, in_mix_ref, docs_ref, arrivals = refs
     x_ref = later[0]
     pairs = [
+        (far_step, log_step_ref),
+        (far_extra, log_extra_ref),
+        (far_docs, docs_ref),
+        (far_later[0], x_ref),
         (far_mix, in_mix_ref),
-        (far_later[0], x_ref),
-        (far_extra, log_extra_ref),
-        (far_step, log_step_ref),
-        (far_docs, docs_ref),
         *zip(far_later[1:], later[1:]),
     ]
     fetches = [
@@ -121,7 +136,7 @@
     ]
     for fetch in fetches:
         fetch.start()
-    for fetch in fetches[:5]:
+    for fetch in fetches[:3]:
         fetch.wait()
     lane = iota((GROUPS, 128), 1)
     fwd = lane < 64
@@ -131,15 +146,17 @@
     turn_ref[0] = cos
     turn_ref[1] = sin
     scale = jnp.sqrt(one_minus_exp(step))
-    wide = iota((ROWS, 128), 1)
-    x = x_ref[...].astype(f32)
-    for g in range(GROUPS):
-        masked[pl.ds(g, ROWS, stride=GROUPS), :] = jnp.where(wide // 16 == g, x, 0.0)
     log_extra = log_extra_ref[...]
     loss = -0.5 * step
     for n in range(ROWS):
         extra = jnp.broadcast_to(log_extra[:, n : n + 1], (GROUPS, 128))
         magnitude[pl.ds(GROUPS * n, GROUPS), :] = jnp.exp(loss + extra)
+    for fetch in fetches[3:5]:
+        fetch.wait()
+    wide = iota((ROWS, 128), 1)
+    x = x_ref[...].astype(f32)
+    for g in range(GROUPS):
+        masked[pl.ds(g, ROWS, stride=GROUPS), :] = jnp.where(wide // 16 == g, x, 0.0)
     mix_real, mix_imag = halves_joined(in_mix_ref[0], in_mix_ref[1])
     rows = masked[...].astype(bf16)
     source[0] = mm(rows, mix_real.astype(bf16))
@@ -166,6 +183,9 @@
             (by_sin * real + new_imag) + by_cos * imag,
         )
         total = total * keep
+        if (n + 1) % (ROWS // SPANS) == 0 and n + 1 < ROWS:
+            for k, reached in enumerate((real, imag, total)):
+                span_ref[n // (ROWS // SPANS), k] = reached
     high = total.astype(bf16).astype(f32)
     low = total - high
     first_doc = docs_ref[0].astype(f32)
@@ -195,7 +215,7 @@
 
 
 def mixer_body(
-    me_ref, messages_ref, real_ref, imag_ref, keep_ref, turn_ref,
+    me_ref, messages_ref, real_ref, imag_ref, keep_ref, turn_ref, span_ref,
     x_ref, read_mix_ref, skip_ref, out_weight_ref,
     partial_ref,
     states, read_out, received, spread,
@@ -204,12 +224,8 @@
     fwd = lane < 64
     me = me_ref[0]
     cos, sin, mine = turn_ref[0], turn_ref[1], turn_ref[2]
-    block_cos, block_sin = cos, sin
-    for _ in range(6):
-        block_cos, block_sin = (
-            block_cos * block_cos - block_sin * block_sin,
-            2.0 * block_cos * block_sin,
-        )
+    span_cos, span_sin = raised(cos, sin, SQUARED)
+    block_cos, block_sin = raised(span_cos, span_sin, 6 - SQUARED)
     received[...] = messages_ref[...].astype(f32)
     place, group = lane & 63, iota((GROUPS, 128), 0)
     of_group = (place == group) | (place == GROUPS + group) | (place == 2 * GROUPS)
@@ -241,19 +257,29 @@
             jnp.where(passed, (by_cos * real + new_real) - by_sin * imag, real),
             jnp.where(passed, (by_sin * real + new_imag) + by_cos * imag, imag),
         )
-    for n in range(ROWS):
-        r = ROWS - 1 - n
-        here, there = pl.ds(GROUPS * n, GROUPS), pl.ds(GROUPS * r, GROUPS)
-        keep = keep_ref[n]
-        by_cos, by_sin = keep * cos, keep * sin
-        real, imag = (
-            (by_cos * real + real_ref[n]) - by_sin * imag,
-            (by_sin * real + imag_ref[n]) + by_cos * imag,
-        )
-        states[0, here, 0:64] = real[:, 0:64]
-        states[0, there, 64:128] = real[:, 64:128]
-        states[1, here, 0:64] = imag[:, 0:64]
-        states[1, there, 64:128] = imag[:, 64:128]
+    span = ROWS // SPANS
+    parts = [(real, imag)]
+    far_cos, far_sin = span_cos, span_sin
+    for q in range(SPANS - 1):
+        total = span_ref[q, 2]
+        parts.append(
+            turned(total * far_cos, total * far_sin, real, imag, span_ref[q, 0], span_ref[q, 1])
+        )
+        far_cos, far_sin = (
+            far_cos * span_cos - far_sin * span_sin,
+            far_cos * span_sin + far_sin * span_cos,
+        )
+    for m in range(span):
+        for q in range(SPANS):
+            n = span * q + m
+            r = ROWS - 1 - n
+            here, there = pl.ds(GROUPS * n, GROUPS), pl.ds(GROUPS * r, GROUPS)
+            keep = keep_ref[n]
+            parts[q] = turned(keep * cos, keep * sin, *parts[q], real_ref[n], imag_ref[n])
+            states[0, here, 0:64] = parts[q][0][:, 0:64]
+            states[0, there, 64:128] = parts[q][0][:, 64:128]
+            states[1, here, 0:64] = parts[q][1][:, 0:64]
+            states[1, there, 64:128] = parts[q][1][:, 64:128]
     read_real, read_imag = halves_joined(read_mix_ref[0], read_mix_ref[1])
     read_out[...] = mm_across(states[0].astype(bf16), read_real.astype(bf16)) + mm_across(
         states[1].astype(bf16), read_imag.astype(bf16)
@@ -314,31 +340,44 @@
 
 
 def copies_body(arrived_ref, gain_ref, copies_ref):
-    rows = mm(packed_rows((EROWS, BLOCKS * PAD), 0), arrived_ref[...]).astype(bf16)
+    row = iota((2 * SENT, BLOCKS * PAD), 0)
+    row = jnp.where(row >= SENT, row - SENT, row)
+    padded = iota((2 * SENT, BLOCKS * PAD), 1)
+    block = divided(padded, PAD)
+    slot = padded - block * PAD
+    packing = (slot < SLOTS) & (row == block * SLOTS + slot)
+    rows = mm(packing.astype(f32).astype(bf16), arrived_ref[...])
     gain = gain_ref[...]
     high = gain.astype(bf16).astype(f32)
     middle = (gain - high).astype(bf16).astype(f32)
     low = gain - high - middle
-    row = iota((16, 128), 0)
-    gains = jnp.where(
-        row == 0, high, jnp.where(row == 1, middle, jnp.where(row == 2, low, 0.0))
-    ).astype(bf16)
-    for j in range(PEERS):
-        copies_ref[j, 0:EROWS, :] = rows
-        copies_ref[j, EROWS:SENT, :] = gains
-
-
-def expert_body(rows_ref, gate_ref, up_ref, down_ref, terms_ref, normed):
+    row = iota((2 * SENT, 128), 0)
+    row = jnp.where(row >= SENT, row - SENT, row) - EROWS
+    for k, part in enumerate((high, middle, low)):
+        rows = jnp.where(row == k, part, rows)
+    rows = rows.astype(bf16)
+    for j in range(PEERS // 2):
+        copies_ref[j] = rows
+
+
+def expert_body(rows_ref, gate_ref, up_ref, down_ref, terms_ref, normed, pieces):
     squares = jnp.zeros((EROWS, 128), f32)
-    for j in range(PEERS):
-        piece = rows_ref[j, 0:EROWS, :].astype(f32)
+    for j in range(PEERS // 2):
+        pieces[j] = rows_ref[j].astype(f32)
+    starts = [(j // 2, SENT * (j % 2)) for j in range(PEERS)]
+    for block, start in starts:
+        piece = pieces[block, start : start + EROWS, :]
         squares = squares + piece * piece
     mean = jnp.sum(squares, axis=1, keepdims=True) / (128 * PEERS)
     factor = lax.rsqrt(mean + epsilon)
-    for j in range(PEERS):
-        gains = rows_ref[j, EROWS:SENT, :].astype(f32)
-        gain = gains[0:1] + gains[1:2] + gains[2:3]
-        piece = rows_ref[j, 0:EROWS, :].astype(f32)
+    for j, (block, start) in enumerate(starts):
+        end = start + EROWS
+        gain = (
+            pieces[block, end : end + 1, :]
+            + pieces[block, end + 1 : end + 2, :]
+            + pieces[block, end + 2 : end + 3, :]
+        )
+        piece = pieces[block, start:end, :]
         normed[:, 128 * j : 128 * (j + 1)] = (piece * factor * gain).astype(bf16)
     rows = normed[...]
     gate = mm(rows, gate_ref[0])
@@ -404,7 +443,7 @@
         route_weight.T,
         norm_gain.reshape(1, 128),
     )
-    message, real, imag, keep, turn, *later = call(
+    message, real, imag, keep, turn, span, *later = call(
         sweep_body,
         [SMEM] + [FAR] * (4 + LATER),
         [
@@ -413,6 +452,7 @@
             ((ROWS, GROUPS, 128), f32),
             ((ROWS, GROUPS, 128), f32),
             ((3, GROUPS, 128), f32),
+            ((SPANS - 1, 3, GROUPS, 128), f32),
             *((x.shape, x.dtype) for x in later),
         ],
         [
@@ -435,7 +475,7 @@
     messages = near(rows_exchanged(message))
     (partial,) = call(
         mixer_body,
-        [SMEM] + [VMEM] * 9,
+        [SMEM] + [VMEM] * 10,
         [((PEERS, ROWS, 128), bf16)],
         [
             ((2, tall, 128), f32),
@@ -444,7 +484,7 @@
             ((BLOCKS * GROUPS, 256), f32),
         ],
     )(
-        me, messages, near(real), near(imag), near(keep), near(turn),
+        me, messages, near(real), near(imag), near(keep), near(turn), near(span),
         mixer_in, read_mix, skip_gain, out_weight,
     )
     shares = near(exchanged(partial, TP))
@@ -454,15 +494,16 @@
         [((ROWS, 128), bf16), ((BLOCKS * PAD, 128), bf16)],
     )(shares, residual, routes)
     arrived = rows_exchanged(outgoing)
-    (copies,) = call(copies_body, [VMEM] * 2, [((PEERS, SENT, 128), bf16)])(
+    (copies,) = call(copies_body, [VMEM] * 2, [((PEERS // 2, 2 * SENT, 128), bf16)])(
         near(arrived), norm_gain
     )
+    gathered = exchanged(copies.reshape(PEERS, SENT // 2, 2, 128), TP).reshape(copies.shape)
     (terms,) = call(
         expert_body,
         [VMEM] * 4,
         [((PEERS, EROWS, 128), bf16)],
-        [((EROWS, 128 * PEERS), bf16)],
-    )(near(exchanged(copies, TP)), switch_matrices, up_weight, down_weight)
+        [((EROWS, 128 * PEERS), bf16), ((PEERS // 2, 2 * SENT, 128), f32)],
+    )(near(gathered), switch_matrices, up_weight, down_weight)
     (answer,) = call(answer_body, [VMEM], [((BLOCKS * PAD, 128), bf16)])(
         near(exchanged(terms, TP))
     )

time: 116 us -> 116 us (level)
  no operation moved by 1% of the time
where the time goes in v6:
time: 116 us
  blocking collectives  110 us (95%)
  Pallas kernels  5.42 us (5%)
    all_to_all x6, blocking collectives, exchanged(): return lax.all_to_all(pieces, axis, 0, 0, tiled=True)  110 us

profile of v6, /device:TPU:1, one launch (start us, length us, event | category | flops | bytes accessed | tf_op | source)
XLA Modules:
  0.0 115.8 jit_solution(18162757448362337918)
XLA Ops:
  0.0 1.9 %shard_map.145 = (bf16[320,128]{1,0:T(8,128)(2,1)S(1)}, f32[64,8,128]{2,1,0:T(8,128)S(1)}, f32[64,8,128]{2,1,0:T(8,128)S(1)}, f32[64,8,128]{2,1,0:T(8,128)S(1)},...) custom-call(s32[1]{0:T(128)} %bitcast.me_ref, ...), custom_call_target="tpu_custom_call" | custom-call | tf_op jit(solution)/shard_map/pallas_call | solution.py:446
  1.9 30.3 %all_to_all.30 = bf16[32,5,2,128]{3,2,1,0:T(2,128)(2,1)S(1)} all-to-all(bf16[32,5,2,128]{3,2,1,0:T(2,128)(2,1)S(1)} %bitcast.24), channel_id=1, replica_groups=mesh['sp'=32,'tp_0'=4,'tp_1'=4] {'sp'}, dimensions={0} | all-to-all | bytes 163840 | tf_op jit(solution)/shard_map/all_to_all | solution.py:409
  32.1 0.0 copy-start.2
  32.1 0.9 shard_map.146
  33.1 14.1 %all_to_all.31.arrived_ref = bf16[16,64,128]{2,1,0:T(8,128)(2,1)S(1)} all-to-all(bf16[16,64,128]{2,1,0:T(8,128)(2,1)S(1)} %shard_map.146), channel_id=1, replica_groups=mesh['sp'=32,'tp_0'=4,'tp_1'=4] {'tp_0','tp_1'}, dimensions={0} | all-to-all | bytes 524288 | tf_op jit(solution)/shard_map/all_to_all | solution.py:409
  47.2 0.2 shard_map.147
  47.5 0.0 copy-start.1
  47.5 18.3 %all_to_all.32 = bf16[32,3,2,128]{3,2,1,0:T(2,128)(2,1)S(1)} all-to-all(bf16[32,3,2,128]{3,2,1,0:T(2,128)(2,1)S(1)} %bitcast.25), channel_id=1, replica_groups=mesh['sp'=32,'tp_0'=4,'tp_1'=4] {'sp'}, dimensions={0} | all-to-all | bytes 98304 | tf_op jit(solution)/shard_map/all_to_all | solution.py:409
  65.7 0.0 copy-start
  65.8 0.2 shard_map.148
  66.0 14.3 %all_to_all.33 = bf16[16,82,2,128]{3,2,1,0:T(2,128)(2,1)S(1)} all-to-all(bf16[16,82,2,128]{3,2,1,0:T(2,128)(2,1)S(1)} %bitcast.19), channel_id=1, replica_groups=mesh['sp'=32,'tp_0'=4,'tp_1'=4] {'tp_0','tp_1'}, dimensions={0} | all-to-all | bytes 1343488 | tf_op jit(solution)/shard_map/all_to_all | solution.py:409
  80.2 0.0 copy-done.2
  80.2 0.0 copy-done.1
  80.2 0.0 copy-done
  80.3 1.0 shard_map.149
  81.3 13.1 %all_to_all.34.terms_ref = bf16[16,160,128]{2,1,0:T(8,128)(2,1)S(1)} all-to-all(bf16[16,160,128]{2,1,0:T(8,128)(2,1)S(1)} %shard_map.149), channel_id=1, replica_groups=mesh['sp'=32,'tp_0'=4,'tp_1'=4] {'tp_0','tp_1'}, dimensions={0} | all-to-all | bytes 1310720 | tf_op jit(solution)/shard_map/all_to_all | solution.py:409
  94.4 0.2 shard_map.150
  94.6 20.2 %all_to_all.35 = bf16[32,3,2,128]{3,2,1,0:T(2,128)(2,1)S(1)} all-to-all(bf16[32,3,2,128]{3,2,1,0:T(2,128)(2,1)S(1)} %bitcast.23), channel_id=1, replica_groups=mesh['sp'=32,'tp_0'=4,'tp_1'=4] {'sp'}, dimensions={0} | all-to-all | bytes 98304 | tf_op jit(solution)/shard_map/all_to_all | solution.py:409
  114.9 0.9 shard_map.151
Async XLA Ops:
  32.1 48.1 %copy-start.2 = (bf16[1,256,2048]{2,1,0:T(8,128)(2,1)S(1)}, bf16[1,256,2048]{2,1,0:T(8,128)(2,1)}, u32[]{:S(2)}) copy-start(bf16[1,256,2048]{2,1,0:T(8,128)(2,1)} %down_ref.1) | copy-start | bytes 3145732
  47.5 32.8 %copy-start.1 = (bf16[1,2048,256]{2,1,0:T(8,128)(2,1)S(1)}, bf16[1,2048,256]{2,1,0:T(8,128)(2,1)}, u32[]{:S(2)}) copy-start(bf16[1,2048,256]{2,1,0:T(8,128)(2,1)} %up_ref.1) | copy-start | bytes 3145732
  65.7 14.5 %copy-start = (bf16[1,2048,256]{2,1,0:T(8,128)(2,1)S(1)}, bf16[1,2048,256]{2,1,0:T(8,128)(2,1)}, u32[]{:S(2)}) copy-start(bf16[1,2048,256]{2,1,0:T(8,128)(2,1)} %gate_ref.1) | copy-start | bytes 3145732

commit v7 on v6

--- a/solution.py
+++ b/solution.py
@@ -27,7 +27,6 @@
 SENT = EROWS + 4
 
 VMEM = pl.BlockSpec(memory_space=pltpu.VMEM)
-SMEM = pl.BlockSpec(memory_space=pltpu.SMEM)
 FAR = pl.BlockSpec(memory_space=pl.ANY if INTERPRET else pltpu.HBM)
 
 
@@ -115,17 +114,20 @@
 
 
 def sweep_body(
-    me_ref, far_docs, far_step, far_extra, far_mix, *refs
+    far_me, far_docs, far_step, far_extra, far_mix, *refs
 ):
     far_later, refs = refs[:LATER], refs[LATER:]
     message_ref, real_ref, imag_ref, keep_ref, turn_ref, span_ref = refs[:6]
     later, refs = refs[6 : 6 + LATER], refs[6 + LATER :]
-    masked, source, magnitude, log_step_ref, log_extra_ref, in_mix_ref, docs_ref, arrivals = refs
+    masked, source, magnitude, log_step_ref, log_extra_ref, in_mix_ref, docs_ref, me_ref, arrivals = (
+        refs
+    )
     x_ref = later[0]
     pairs = [
         (far_step, log_step_ref),
         (far_extra, log_extra_ref),
         (far_docs, docs_ref),
+        (far_me, me_ref),
         (far_later[0], x_ref),
         (far_mix, in_mix_ref),
         *zip(far_later[1:], later[1:]),
@@ -136,7 +138,7 @@
     ]
     for fetch in fetches:
         fetch.start()
-    for fetch in fetches[:3]:
+    for fetch in fetches[:4]:
         fetch.wait()
     lane = iota((GROUPS, 128), 1)
     fwd = lane < 64
@@ -151,7 +153,7 @@
     for n in range(ROWS):
         extra = jnp.broadcast_to(log_extra[:, n : n + 1], (GROUPS, 128))
         magnitude[pl.ds(GROUPS * n, GROUPS), :] = jnp.exp(loss + extra)
-    for fetch in fetches[3:5]:
+    for fetch in fetches[4:6]:
         fetch.wait()
     wide = iota((ROWS, 128), 1)
     x = x_ref[...].astype(f32)
@@ -191,6 +193,7 @@
     first_doc = docs_ref[0].astype(f32)
     last_doc = docs_ref[ROWS - 1].astype(f32)
     turn_ref[2] = jnp.where(fwd, first_doc, last_doc)
+    turn_ref[3] = jnp.broadcast_to(me_ref[0].astype(f32), (GROUPS, 128))
     group = iota((GROUPS, 128), 0)
     lines = []
     for kept, doc, left, right in [
@@ -210,20 +213,19 @@
     receiver = divided(row, LINES)
     wanted = row - receiver * LINES + jnp.where(receiver > me_ref[0], 0, 16)
     message_ref[...] = mm((entry == wanted).astype(f32).astype(bf16), lines).astype(bf16)
-    for fetch in fetches[5:]:
+    for fetch in fetches[6:]:
         fetch.wait()
 
 
 def mixer_body(
-    me_ref, messages_ref, real_ref, imag_ref, keep_ref, turn_ref, span_ref,
+    messages_ref, real_ref, imag_ref, keep_ref, turn_ref, span_ref,
     x_ref, read_mix_ref, skip_ref, out_weight_ref,
     partial_ref,
     states, read_out, received, spread,
 ):
     lane = iota((GROUPS, 128), 1)
     fwd = lane < 64
-    me = me_ref[0]
-    cos, sin, mine = turn_ref[0], turn_ref[1], turn_ref[2]
+    cos, sin, mine, me = turn_ref[0], turn_ref[1], turn_ref[2], turn_ref[3]
     span_cos, span_sin = raised(cos, sin, SQUARED)
     block_cos, block_sin = raised(span_cos, span_sin, 6 - SQUARED)
     received[...] = messages_ref[...].astype(f32)
@@ -252,7 +254,7 @@
         new_real = jnp.where(same, jnp.where(fwd, one, two), 0.0)
         new_imag = jnp.where(same, pltpu.roll(jnp.where(fwd, two, one), 64, 1), 0.0)
         by_cos, by_sin = decay * block_cos, decay * block_sin
-        passed = jnp.where(fwd, (n < me).astype(jnp.int32), (r > me).astype(jnp.int32)) > 0
+        passed = (fwd & (me > n)) | (~fwd & (me < r))
         real, imag = (
             jnp.where(passed, (by_cos * real + new_real) - by_sin * imag, real),
             jnp.where(passed, (by_sin * real + new_imag) + by_cos * imag, imag),
@@ -445,13 +447,13 @@
     )
     message, real, imag, keep, turn, span, *later = call(
         sweep_body,
-        [SMEM] + [FAR] * (4 + LATER),
+        [FAR] * (5 + LATER),
         [
             ((BLOCKS * LINES, 128), bf16),
             ((ROWS, GROUPS, 128), f32),
             ((ROWS, GROUPS, 128), f32),
             ((ROWS, GROUPS, 128), f32),
-            ((3, GROUPS, 128), f32),
+            ((4, GROUPS, 128), f32),
             ((SPANS - 1, 3, GROUPS, 128), f32),
             *((x.shape, x.dtype) for x in later),
         ],
@@ -463,10 +465,11 @@
             ((GROUPS, ROWS), f32),
             ((2, 128, 128), f32),
             ((ROWS,), jnp.int32),
+            ((1,), jnp.int32),
         ],
-        copies=4 + LATER,
+        copies=5 + LATER,
     )(
-        me, far(doc_ids), far(log_step), far(log_extra.T), far(in_mix.reshape(2, 128, 128)),
+        far(me), far(doc_ids), far(log_step), far(log_extra.T), far(in_mix.reshape(2, 128, 128)),
         *map(far, later),
     )
     mixer_in, read_mix, skip_gain, out_weight, residual, routes, route_weight, norm_gain = map(
@@ -475,7 +478,7 @@
     messages = near(rows_exchanged(message))
     (partial,) = call(
         mixer_body,
-        [SMEM] + [VMEM] * 10,
+        [VMEM] * 10,
         [((PEERS, ROWS, 128), bf16)],
         [
             ((2, tall, 128), f32),
@@ -484,7 +487,7 @@
             ((BLOCKS * GROUPS, 256), f32),
         ],
     )(
-        me, messages, near(real), near(imag), near(keep), near(turn), near(span),
+        messages, near(real), near(imag), near(keep), near(turn), near(span),
         mixer_in, read_mix, skip_gain, out_weight,
     )
     shares = near(exchanged(partial, TP))

time: 116 us -> 116 us (level)
  no operation moved by 1% of the time
where the time goes in v7:
time: 116 us
  blocking collectives  110 us (95%)
  Pallas kernels  5.45 us (5%)
    all_to_all x6, blocking collectives, exchanged(): return lax.all_to_all(pieces, axis, 0, 0, tiled=True)  110 us

profile of v7, /device:TPU:1, one launch (start us, length us, event | category | flops | bytes accessed | tf_op | source)
XLA Modules:
  0.0 115.8 jit_solution(56218410026255641)
XLA Ops:
  0.0 1.9 %shard_map.145 = (bf16[320,128]{1,0:T(8,128)(2,1)S(1)}, f32[64,8,128]{2,1,0:T(8,128)S(1)}, f32[64,8,128]{2,1,0:T(8,128)S(1)}, f32[64,8,128]{2,1,0:T(8,128)S(1)},...) custom-call(s32[1]{0:T(128)} %bitcast.far_me, ...), custom_call_target="tpu_custom_call" | custom-call | tf_op jit(solution)/shard_map/pallas_call | solution.py:448
  1.9 30.3 %all_to_all.30 = bf16[32,5,2,128]{3,2,1,0:T(2,128)(2,1)S(1)} all-to-all(bf16[32,5,2,128]{3,2,1,0:T(2,128)(2,1)S(1)} %bitcast.24), channel_id=1, replica_groups=mesh['sp'=32,'tp_0'=4,'tp_1'=4] {'sp'}, dimensions={0} | all-to-all | bytes 163840 | tf_op jit(solution)/shard_map/all_to_all | solution.py:411
  32.1 0.0 copy-start.2
  32.1 0.9 shard_map.146
  33.1 14.1 %all_to_all.31.arrived_ref = bf16[16,64,128]{2,1,0:T(8,128)(2,1)S(1)} all-to-all(bf16[16,64,128]{2,1,0:T(8,128)(2,1)S(1)} %shard_map.146), channel_id=1, replica_groups=mesh['sp'=32,'tp_0'=4,'tp_1'=4] {'tp_0','tp_1'}, dimensions={0} | all-to-all | bytes 524288 | tf_op jit(solution)/shard_map/all_to_all | solution.py:411
  47.2 0.2 shard_map.147
  47.5 0.0 copy-start.1
  47.5 18.3 %all_to_all.32 = bf16[32,3,2,128]{3,2,1,0:T(2,128)(2,1)S(1)} all-to-all(bf16[32,3,2,128]{3,2,1,0:T(2,128)(2,1)S(1)} %bitcast.25), channel_id=1, replica_groups=mesh['sp'=32,'tp_0'=4,'tp_1'=4] {'sp'}, dimensions={0} | all-to-all | bytes 98304 | tf_op jit(solution)/shard_map/all_to_all | solution.py:411
  65.8 0.0 copy-start
  65.8 0.2 shard_map.148
  66.0 14.3 %all_to_all.33 = bf16[16,82,2,128]{3,2,1,0:T(2,128)(2,1)S(1)} all-to-all(bf16[16,82,2,128]{3,2,1,0:T(2,128)(2,1)S(1)} %bitcast.19), channel_id=1, replica_groups=mesh['sp'=32,'tp_0'=4,'tp_1'=4] {'tp_0','tp_1'}, dimensions={0} | all-to-all | bytes 1343488 | tf_op jit(solution)/shard_map/all_to_all | solution.py:411
  80.3 0.0 copy-done.2
  80.3 0.0 copy-done.1
  80.3 0.0 copy-done
  80.3 1.0 shard_map.149
  81.3 13.1 %all_to_all.34.terms_ref = bf16[16,160,128]{2,1,0:T(8,128)(2,1)S(1)} all-to-all(bf16[16,160,128]{2,1,0:T(8,128)(2,1)S(1)} %shard_map.149), channel_id=1, replica_groups=mesh['sp'=32,'tp_0'=4,'tp_1'=4] {'tp_0','tp_1'}, dimensions={0} | all-to-all | bytes 1310720 | tf_op jit(solution)/shard_map/all_to_all | solution.py:411
  94.4 0.2 shard_map.150
  94.7 20.2 %all_to_all.35 = bf16[32,3,2,128]{3,2,1,0:T(2,128)(2,1)S(1)} all-to-all(bf16[32,3,2,128]{3,2,1,0:T(2,128)(2,1)S(1)} %bitcast.23), channel_id=1, replica_groups=mesh['sp'=32,'tp_0'=4,'tp_1'=4] {'sp'}, dimensions={0} | all-to-all | bytes 98304 | tf_op jit(solution)/shard_map/all_to_all | solution.py:411
  114.9 0.9 shard_map.151
Async XLA Ops:
  32.1 48.1 %copy-start.2 = (bf16[1,256,2048]{2,1,0:T(8,128)(2,1)S(1)}, bf16[1,256,2048]{2,1,0:T(8,128)(2,1)}, u32[]{:S(2)}) copy-start(bf16[1,256,2048]{2,1,0:T(8,128)(2,1)} %down_ref.1) | copy-start | bytes 3145732
  47.5 32.8 %copy-start.1 = (bf16[1,2048,256]{2,1,0:T(8,128)(2,1)S(1)}, bf16[1,2048,256]{2,1,0:T(8,128)(2,1)}, u32[]{:S(2)}) copy-start(bf16[1,2048,256]{2,1,0:T(8,128)(2,1)} %up_ref.1) | copy-start | bytes 3145732
  65.8 14.5 %copy-start = (bf16[1,2048,256]{2,1,0:T(8,128)(2,1)S(1)}, bf16[1,2048,256]{2,1,0:T(8,128)(2,1)}, u32[]{:S(2)}) copy-start(bf16[1,2048,256]{2,1,0:T(8,128)(2,1)} %gate_ref.1) | copy-start | bytes 3145732

commit v8 on v6

--- a/solution.py
+++ b/solution.py
@@ -136,7 +136,7 @@
     ]
     for fetch in fetches:
         fetch.start()
-    for fetch in fetches[:3]:
+    for fetch in fetches[:5]:
         fetch.wait()
     lane = iota((GROUPS, 128), 1)
     fwd = lane < 64
@@ -151,13 +151,15 @@
     for n in range(ROWS):
         extra = jnp.broadcast_to(log_extra[:, n : n + 1], (GROUPS, 128))
         magnitude[pl.ds(GROUPS * n, GROUPS), :] = jnp.exp(loss + extra)
-    for fetch in fetches[3:5]:
-        fetch.wait()
     wide = iota((ROWS, 128), 1)
     x = x_ref[...].astype(f32)
     for g in range(GROUPS):
         masked[pl.ds(g, ROWS, stride=GROUPS), :] = jnp.where(wide // 16 == g, x, 0.0)
     mix_real, mix_imag = halves_joined(in_mix_ref[0], in_mix_ref[1])
+    scales = jnp.concatenate(
+        [jnp.broadcast_to(scale[g : g + 1, :], (16, 128)) for g in range(GROUPS)], axis=0
+    )
+    mix_real, mix_imag = mix_real * scales, mix_imag * scales
     rows = masked[...].astype(bf16)
     source[0] = mm(rows, mix_real.astype(bf16))
     source[1] = mm(rows, mix_imag.astype(bf16))
@@ -172,8 +174,8 @@
             same_fwd = jnp.where(docs_ref[n] == docs_ref[n - 1], 1.0, 0.0)
             same_bwd = jnp.where(docs_ref[r] == docs_ref[r + 1], 1.0, 0.0)
             keep = keep * jnp.where(fwd, same_fwd, same_bwd)
-        new_real = scale * jnp.where(fwd, source[0, here, :], source[0, there, :])
-        new_imag = scale * jnp.where(fwd, source[1, here, :], source[1, there, :])
+        new_real = jnp.where(fwd, source[0, here, :], source[0, there, :])
+        new_imag = jnp.where(fwd, source[1, here, :], source[1, there, :])
         keep_ref[n] = keep
         real_ref[n] = new_real
         imag_ref[n] = new_imag

time: 116 us -> 116 us (level)
  no operation moved by 1% of the time
where the time goes in v8:
time: 116 us
  blocking collectives  110 us (95%)
  Pallas kernels  5.45 us (5%)
    all_to_all x6, blocking collectives, exchanged(): return lax.all_to_all(pieces, axis, 0, 0, tiled=True)  110 us

profile of v8, /device:TPU:1, one launch (start us, length us, event | category | flops | bytes accessed | tf_op | source)
XLA Modules:
  0.0 115.8 jit_solution(8025637952216706132)
XLA Ops:
  0.0 1.9 %shard_map.145 = (bf16[320,128]{1,0:T(8,128)(2,1)S(1)}, f32[64,8,128]{2,1,0:T(8,128)S(1)}, f32[64,8,128]{2,1,0:T(8,128)S(1)}, f32[64,8,128]{2,1,0:T(8,128)S(1)},...) custom-call(s32[1]{0:T(128)} %bitcast.me_ref, ...), custom_call_target="tpu_custom_call" | custom-call | tf_op jit(solution)/shard_map/pallas_call | solution.py:448
  1.9 30.3 %all_to_all.30 = bf16[32,5,2,128]{3,2,1,0:T(2,128)(2,1)S(1)} all-to-all(bf16[32,5,2,128]{3,2,1,0:T(2,128)(2,1)S(1)} %bitcast.24), channel_id=1, replica_groups=mesh['sp'=32,'tp_0'=4,'tp_1'=4] {'sp'}, dimensions={0} | all-to-all | bytes 163840 | tf_op jit(solution)/shard_map/all_to_all | solution.py:411
  32.1 0.0 copy-start.2
  32.1 0.9 shard_map.146
  33.1 14.1 %all_to_all.31.arrived_ref = bf16[16,64,128]{2,1,0:T(8,128)(2,1)S(1)} all-to-all(bf16[16,64,128]{2,1,0:T(8,128)(2,1)S(1)} %shard_map.146), channel_id=1, replica_groups=mesh['sp'=32,'tp_0'=4,'tp_1'=4] {'tp_0','tp_1'}, dimensions={0} | all-to-all | bytes 524288 | tf_op jit(solution)/shard_map/all_to_all | solution.py:411
  47.2 0.2 shard_map.147
  47.5 0.0 copy-start.1
  47.5 18.3 %all_to_all.32 = bf16[32,3,2,128]{3,2,1,0:T(2,128)(2,1)S(1)} all-to-all(bf16[32,3,2,128]{3,2,1,0:T(2,128)(2,1)S(1)} %bitcast.25), channel_id=1, replica_groups=mesh['sp'=32,'tp_0'=4,'tp_1'=4] {'sp'}, dimensions={0} | all-to-all | bytes 98304 | tf_op jit(solution)/shard_map/all_to_all | solution.py:411
  65.8 0.0 copy-start
  65.8 0.2 shard_map.148
  66.0 14.3 %all_to_all.33 = bf16[16,82,2,128]{3,2,1,0:T(2,128)(2,1)S(1)} all-to-all(bf16[16,82,2,128]{3,2,1,0:T(2,128)(2,1)S(1)} %bitcast.19), channel_id=1, replica_groups=mesh['sp'=32,'tp_0'=4,'tp_1'=4] {'tp_0','tp_1'}, dimensions={0} | all-to-all | bytes 1343488 | tf_op jit(solution)/shard_map/all_to_all | solution.py:411
  80.3 0.0 copy-done.2
  80.3 0.0 copy-done.1
  80.3 0.0 copy-done
  80.3 1.0 shard_map.149
  81.3 13.1 %all_to_all.34.terms_ref = bf16[16,160,128]{2,1,0:T(8,128)(2,1)S(1)} all-to-all(bf16[16,160,128]{2,1,0:T(8,128)(2,1)S(1)} %shard_map.149), channel_id=1, replica_groups=mesh['sp'=32,'tp_0'=4,'tp_1'=4] {'tp_0','tp_1'}, dimensions={0} | all-to-all | bytes 1310720 | tf_op jit(solution)/shard_map/all_to_all | solution.py:411
  94.4 0.2 shard_map.150
  94.7 20.2 %all_to_all.35 = bf16[32,3,2,128]{3,2,1,0:T(2,128)(2,1)S(1)} all-to-all(bf16[32,3,2,128]{3,2,1,0:T(2,128)(2,1)S(1)} %bitcast.23), channel_id=1, replica_groups=mesh['sp'=32,'tp_0'=4,'tp_1'=4] {'sp'}, dimensions={0} | all-to-all | bytes 98304 | tf_op jit(solution)/shard_map/all_to_all | solution.py:411
  114.9 0.9 shard_map.151
Async XLA Ops:
  32.1 48.1 %copy-start.2 = (bf16[1,256,2048]{2,1,0:T(8,128)(2,1)S(1)}, bf16[1,256,2048]{2,1,0:T(8,128)(2,1)}, u32[]{:S(2)}) copy-start(bf16[1,256,2048]{2,1,0:T(8,128)(2,1)} %down_ref.1) | copy-start | bytes 3145732
  47.5 32.8 %copy-start.1 = (bf16[1,2048,256]{2,1,0:T(8,128)(2,1)S(1)}, bf16[1,2048,256]{2,1,0:T(8,128)(2,1)}, u32[]{:S(2)}) copy-start(bf16[1,2048,256]{2,1,0:T(8,128)(2,1)} %up_ref.1) | copy-start | bytes 3145732
  65.8 14.5 %copy-start = (bf16[1,2048,256]{2,1,0:T(8,128)(2,1)S(1)}, bf16[1,2048,256]{2,1,0:T(8,128)(2,1)}, u32[]{:S(2)}) copy-start(bf16[1,2048,256]{2,1,0:T(8,128)(2,1)} %gate_ref.1) | copy-start | bytes 3145732
